TPU v7x, 32 devices: a whole 2x2x4 slice. The times are simulated.
32 devices in a mesh: rep: 2 (over x), fs: 8 (over z, y), tp: 2 (over core).
Axes of the slice: x: 2, y: 2, z: 4, core: 2. Of those that a mesh axis runs over, the one named last changes fastest.
Arguments:
- x_later: bfloat16 [2048, 2048], P(('rep', 'fs')), may hold values from -6 to 6
- kept_input_rows: bfloat16 [2048, 2048], P(('rep', 'fs')), may hold values from -6 to 6
- cotangent: bfloat16 [2048, 2048], P(('rep', 'fs')), may hold values from -8 to 8
- norm_gain_vector: float32 [2048], replicated, may hold values from 0.1 to 1.9
- up_weight: bfloat16 [2048, 4096], P('fs', 'tp'), may hold values from -0.125 to 0.125
- down_weight: bfloat16 [4096, 2048], P('tp', 'fs'), may hold values from -0.09375 to 0.09375
- up_sum: float32 [2048, 4096], P('fs', 'tp'), may hold values from -6 to 6
- down_sum: float32 [4096, 2048], P('tp', 'fs'), may hold values from -6 to 6
Outputs:
- mixed: bfloat16 [2048, 2048], P(('rep', 'fs'))
- input_gradient_rows: bfloat16 [2048, 2048], P(('rep', 'fs'))
- up_total: float32 [2048, 4096], P('fs', 'tp')
- down_total: float32 [4096, 2048], P('tp', 'fs')
All inputs are finite; a program needn't handle non-finite values.
Results may differ from a plain program's by a relative error of at most 0.018.
Values may be sent and summed in bfloat16 or wider, within the bound.
A program may use at most 128 MiB of HBM per device.

v0:
```python
import jax
import jax.numpy as jnp
from jax import lax
from jax.sharding import PartitionSpec as P

EPSILON = 1e-06
TRANSPOSED = (((1,), (1,)), ((), ()))
LEADING = (((0,), (0,)), ((), ()))


def norm_partial_terms(values, norm_gain_vector):
    floats = values.astype(jnp.float32)
    inverse = lax.rsqrt(jnp.mean(floats * floats, axis=-1, keepdims=True) + EPSILON)
    unit_rows = floats * inverse
    normed = (unit_rows * norm_gain_vector).astype(jnp.bfloat16)
    return (inverse, unit_rows, normed)


def squared_relu(pre_act):
    return jnp.square(jax.nn.relu(pre_act)).astype(jnp.bfloat16)


def body(
    x_later, kept_input_rows, cotangent, norm_gain_vector, up_weight, down_weight, up_sum, down_sum
):
    row_count = x_later.shape[0]
    grad_scale = float(row_count * lax.axis_size("rep") * lax.axis_size("fs")) ** (-0.5)
    inv_later, unit_later, normed_later = norm_partial_terms(x_later, norm_gain_vector)
    inverse_rms_kept, unit_kept_rows, normed_kept_rows = norm_partial_terms(
        kept_input_rows, norm_gain_vector
    )
    stacked = jnp.concatenate([normed_kept_rows, normed_later], axis=0)
    up_whole = lax.all_gather(up_weight, "fs", axis=0, tiled=True)
    down_whole = lax.all_gather(down_weight, "fs", axis=1, tiled=True)
    pre_act = jnp.dot(stacked, up_whole, preferred_element_type=jnp.float32)
    pre_saved = pre_act[:row_count]
    hidden_saved = squared_relu(pre_saved)
    hidden_later = squared_relu(pre_act[row_count:])
    mixed_part = jnp.dot(hidden_later, down_whole, preferred_element_type=jnp.float32)
    hidden_grad = lax.dot_general(
        cotangent, down_whole, TRANSPOSED, preferred_element_type=jnp.float32
    )
    pre_grad = (hidden_grad * 2.0 * jax.nn.relu(pre_saved)).astype(jnp.bfloat16)
    back_part = lax.dot_general(pre_grad, up_whole, TRANSPOSED, preferred_element_type=jnp.float32)
    mixed_sum, back_sum = (
        lax.psum(mixed_part.astype(jnp.bfloat16), "tp").astype(jnp.float32),
        lax.psum(back_part.astype(jnp.bfloat16), "tp").astype(jnp.float32),
    )
    mixed = mixed_sum.astype(jnp.bfloat16)
    scaled_rows = back_sum * norm_gain_vector
    input_gradient_rows = (
        inverse_rms_kept
        * (
            scaled_rows
            - unit_kept_rows * jnp.mean(scaled_rows * unit_kept_rows, axis=-1, keepdims=True)
        )
    ).astype(jnp.bfloat16)
    cot_columns, normed_columns = (
        lax.all_to_all(cotangent, "fs", split_axis=1, concat_axis=0, tiled=True),
        lax.all_to_all(normed_kept_rows, "fs", split_axis=1, concat_axis=0, tiled=True),
    )
    columns = normed_columns
    up_grad = grad_scale * lax.dot_general(
        columns,
        lax.all_gather(pre_grad, "fs", axis=0, tiled=True),
        LEADING,
        preferred_element_type=jnp.float32,
    )
    columns = cot_columns
    down_grad = lax.dot_general(
        lax.all_gather(hidden_saved, "fs", axis=0, tiled=True),
        columns,
        LEADING,
        preferred_element_type=jnp.float32,
    )
    up_added, down_added = (
        lax.psum(up_grad.astype(jnp.bfloat16), "rep").astype(jnp.float32),
        lax.psum((down_grad * grad_scale).astype(jnp.bfloat16), "rep").astype(jnp.float32),
    )
    return (mixed, input_gradient_rows, up_sum + up_added, down_sum + down_added)


def solution(mesh):
    return jax.shard_map(
        body,
        mesh=mesh,
        in_specs=(
            P(("rep", "fs"), None),
            P(("rep", "fs"), None),
            P(("rep", "fs"), None),
            P(),
            P("fs", "tp"),
            P("tp", "fs"),
            P("fs", "tp"),
            P("tp", "fs"),
        ),
        out_specs=(P(("rep", "fs"), None), P(("rep", "fs"), None), P("fs", "tp"), P("tp", "fs")),
        check_vma=False,
    )
```

profile of v0, /device:TPU:11, one launch (start us, length us, event | category | flops | bytes accessed | tf_op | source)
XLA Modules:
  0.0 527.1 jit_solution(5209022725522216532)
XLA Ops:
  7.2 0.0 copy-start
  7.2 0.0 copy-start.5
  7.2 0.0 copy-start.8
  7.2 0.0 all-gather.5.cloned.1.call-start
  7.2 0.7 all-gather.5.cloned.1.call-update
  7.9 0.0 all-gather.7.cloned.1.call-start
  8.0 0.7 all-gather.7.cloned.1.call-update
  8.7 0.0 all-gather.9.cloned.1.call-start
  8.7 0.0 copy-done
  8.7 0.2 fusion.12
  8.9 0.0 copy-done.5
  8.9 0.2 fusion.13
  9.1 0.0 copy-done.8
  9.1 1.3 fusion.7
  10.4 122.8 %all-gather.5.cloned.1.call-done = bf16[2048,2048]{1,0:T(8,128)(2,1)} async-done(((bf16[256,2048]{1,0:T(8,128)(2,1)}), bf16[2048,2048]{1,0:T(8,128)(2,1)}) %all-gather.5.cloned.1.call-update) | async-done | bytes 8388624 | tf_op jit(solution)/shard_map/all_gather | solution.py:33
  133.2 0.0 copy-start.2
  133.2 6.1 %fusion.18 = f32[256,2048]{1,0:T(8,128)S(1)} fusion(bf16[2048,2048]{1,0:T(8,128)(2,1)} %all-gather.5.cloned.1.call-done, bf16[128,2048]{1,0:T(8,128)(2,1)} %get-tuple-element.9, bf16[128,2048]{1,0:T(8,128)(2,1)} %get-tuple-element.8), kind=kOutput, calls=%fused_computation.31 | convolution fusion | flops 2149580800 | bytes 11534336 | tf_op jit(solution)/shard_map/dot_general | solution.py:35
  139.3 119.1 %all-gather.7.cloned.1.call-done = bf16[2048,2048]{1,0:T(8,128)(2,1)} async-done(((bf16[2048,256]{1,0:T(8,128)(2,1)}), bf16[2048,2048]{1,0:T(8,128)(2,1)}) %all-gather.7.cloned.1.call-update) | async-done | bytes 8388624 | tf_op jit(solution)/shard_map/all_gather | solution.py:34
  258.4 0.0 copy-done.2
  258.4 7.1 %fusion.3 = bf16[128,2048]{1,0:T(8,128)(2,1)} fusion(bf16[128,2048]{1,0:T(8,128)(2,1)S(1)} %copy-done.2, bf16[2048,2048]{1,0:T(8,128)(2,1)} %all-gather.7.cloned.1.call-done, f32[256,2048]{1,0:T(8,128)S(1)} %fusion.18), kind=kOutput, calls=%fused_computation.8 | convolution fusion | flops 1074790400 | bytes 10485760 | tf_op jit(solution)/shard_map/dot_general | solution.py:40
  265.5 0.0 all-gather.9.cloned.1.call-update
  265.5 0.0 all-gather.11.cloned.1.call-start
  265.5 0.9 multiply_convert_fusion
  266.4 0.0 all-gather.11.cloned.1.call-update
  266.5 0.0 copy-start.1
  266.5 2.2 copy.14
  268.6 6.2 %all-to-all-start.1 = ((bf16[128,8,256]{0,2,1:T(8,128)(2,1)}), bf16[128,8,256]{0,2,1:T(8,128)(2,1)}, u32[]{:S(2)}, u32[]{:S(2)}) async-start(bf16[128,8,256]{0,2,1:T(8,128)(2,1)} %bitcast.21), calls=%async_computation.1 | async-start | bytes 1048576 | tf_op jit(solution)/shard_map/all_to_all | solution.py:59
  274.8 1.9 copy.18
  276.7 21.9 %all-to-all-done.1 = bf16[128,8,256]{0,2,1:T(8,128)(2,1)} async-done(((bf16[128,8,256]{0,2,1:T(8,128)(2,1)}), bf16[128,8,256]{0,2,1:T(8,128)(2,1)}, u32[]{:S(2)}, u32[]{:S(2)}) %all-to-all-start.1) | async-done | bytes 524320 | tf_op jit(solution)/shard_map/all_to_all | solution.py:59
  298.6 6.3 %all-to-all-start = ((bf16[128,8,256]{2,0,1:T(8,128)(2,1)}), bf16[128,8,256]{2,0,1:T(8,128)(2,1)}, u32[]{:S(2)}, u32[]{:S(2)}) async-start(bf16[128,8,256]{2,0,1:T(8,128)(2,1)} %bitcast.20), calls=%async_computation | async-start | bytes 1048576 | tf_op jit(solution)/shard_map/all_to_all | solution.py:60
  304.9 0.0 all-reduce.5.cloned.1.call-start
  304.9 0.0 copy-done.1
  304.9 7.1 %convolution_convert_fusion = bf16[128,2048]{1,0:T(8,128)(2,1)} fusion(bf16[128,2048]{1,0:T(8,128)(2,1)S(1)} %copy-done.1, bf16[2048,2048]{1,0:T(8,128)(2,1)} %all-gather.5.cloned.1.call-done), kind=kOutput, calls=%fused_computation.6 | convolution fusion | flops 1074003968 | bytes 9437184 | tf_op jit(solution)/shard_map/dot_general | solution.py:44
  312.1 5.5 %convolution_convert_fusion.1 = bf16[128,2048]{1,0:T(8,128)(2,1)} fusion(bf16[2048,2048]{1,0:T(8,128)(2,1)} %all-gather.7.cloned.1.call-done, f32[256,2048]{1,0:T(8,128)S(1)} %fusion.18), kind=kOutput, calls=%fused_computation.7 | convolution fusion | flops 1074790400 | bytes 9961472 | tf_op jit(solution)/shard_map/dot_general | solution.py:39
  317.6 0.0 all-reduce.5.cloned.1.call-update
  317.6 0.2 all-reduce.7.cloned.1.call-start
  317.8 1.2 copy.15
  319.1 0.3 all-to-all-done
  319.4 31.9 %all-gather.9.cloned.1.call-done = bf16[1024,2048]{1,0:T(8,128)(2,1)} async-done(((bf16[128,2048]{1,0:T(8,128)(2,1)}), bf16[1024,2048]{1,0:T(8,128)(2,1)}) %all-gather.9.cloned.1.call-update) | async-done | bytes 4194320 | tf_op jit(solution)/shard_map/all_gather | solution.py:65
  351.3 4.6 fusion
  355.9 70.2 %all-gather.11.cloned.1.call-done = bf16[1024,2048]{1,0:T(8,128)(2,1)} async-done(((bf16[128,2048]{1,0:T(8,128)(2,1)}), bf16[1024,2048]{1,0:T(8,128)(2,1)}) %all-gather.11.cloned.1.call-update) | async-done | bytes 4194320 | tf_op jit(solution)/shard_map/all_gather | solution.py:71
  426.1 4.5 fusion.1
  430.6 0.0 copy-start.3
  430.6 0.0 all-reduce.7.cloned.1.call-update
  430.6 19.1 %all-reduce.5.cloned.1.call-done = (bf16[128,2048]{1,0:T(8,128)(2,1)}, bf16[128,2048]{1,0:T(8,128)(2,1)}) async-done(((bf16[128,2048]{1,0:T(8,128)(2,1)}, bf16[128,2048]{1,0:T(8,128)(2,1)}), (bf16[128,2048]{1,0:T(8,128)(2,1)}, bf16[128,2048]{1,0:T(8,128)(2,1)})) %all-reduce.5.cloned.1.call-update) | async-done | bytes 1048592 | tf_op jit(solution)/shard_map/psum | solution.py:46
  449.7 1.4 fusion.8
  451.1 2.2 fusion.11
  453.3 61.6 %all-reduce.7.cloned.1.call-done = (bf16[256,2048]{1,0:T(8,128)(2,1)}, bf16[2048,256]{1,0:T(8,128)(2,1)}) async-done(((bf16[256,2048]{1,0:T(8,128)(2,1)}, bf16[2048,256]{1,0:T(8,128)(2,1)}), (bf16[256,2048]{1,0:T(8,128)(2,1)}, bf16[2048,256]{1,0:T(8,128)(2,1)})) %all-reduce.7.cloned.1.call-update) | async-done | bytes 2097168 | tf_op jit(solution)/shard_map/psum | solution.py:77
  514.9 0.0 copy-done.3
  514.9 0.0 copy-start.4
  514.9 0.0 copy-start.6
  514.9 2.9 convert_add_fusion
  517.8 0.0 copy-done.4
  517.8 0.0 copy-done.6
  517.8 0.0 copy-start.7
  517.8 1.6 convert_add_fusion.1
  519.4 0.0 copy-done.7
  519.4 0.8 copy.23
  (2 shorter events, 0.0 us)
Async XLA Ops:
  7.2 1.6 copy-start
  7.2 1.8 copy-start.5
  7.2 1.9 copy-start.8
  7.2 126.0 %all-gather.5.cloned.1.call-start = ((), (), s32[]{:S(2)}) async-start(), calls=%async_computation.2 | async-start | bytes 9437184 | tf_op jit(solution)/shard_map/all_gather | solution.py:33
  7.9 250.5 %all-gather.7.cloned.1.call-start = ((), (), s32[]{:S(2)}) async-start(), calls=%async_computation.3 | async-start | bytes 9437184 | tf_op jit(solution)/shard_map/all_gather | solution.py:34
  8.7 342.6 %all-gather.9.cloned.1.call-start = ((), (), s32[]{:S(2)}) async-start(), calls=%async_computation.4 | async-start | bytes 4718592 | tf_op jit(solution)/shard_map/all_gather | solution.py:65
  133.2 125.2 %copy-start.2 = (bf16[128,2048]{1,0:T(8,128)(2,1)S(1)}, bf16[128,2048]{1,0:T(8,128)(2,1)}, u32[]{:S(2)}) copy-start(bf16[128,2048]{1,0:T(8,128)(2,1)} %param.10) | copy-start | bytes 1572868
  265.5 160.6 %all-gather.11.cloned.1.call-start = ((), (), s32[]{:S(2)}) async-start(), calls=%async_computation.5 | async-start | bytes 4718592 | tf_op jit(solution)/shard_map/all_gather | solution.py:71
  266.5 38.5 %copy-start.1 = (bf16[128,2048]{1,0:T(8,128)(2,1)S(1)}, bf16[128,2048]{1,0:T(8,128)(2,1)}, u32[]{:S(2)}) copy-start(bf16[128,2048]{1,0:T(8,128)(2,1)} %fusion.3) | copy-start | bytes 1572868
  268.6 30.0 %all-to-all-start.1 = ((bf16[128,8,256]{0,2,1:T(8,128)(2,1)}), bf16[128,8,256]{0,2,1:T(8,128)(2,1)}, u32[]{:S(2)}, u32[]{:S(2)}) async-start(bf16[128,8,256]{0,2,1:T(8,128)(2,1)} %bitcast.21), calls=%async_computation.1 | async-start | bytes 1048576 | tf_op jit(solution)/shard_map/all_to_all | solution.py:59
  298.6 20.7 %all-to-all-start = ((bf16[128,8,256]{2,0,1:T(8,128)(2,1)}), bf16[128,8,256]{2,0,1:T(8,128)(2,1)}, u32[]{:S(2)}, u32[]{:S(2)}) async-start(bf16[128,8,256]{2,0,1:T(8,128)(2,1)} %bitcast.20), calls=%async_computation | async-start | bytes 1048576 | tf_op jit(solution)/shard_map/all_to_all | solution.py:60
  304.9 144.8 %all-reduce.5.cloned.1.call-start = ((), (), s32[]{:S(2)}) async-start(), calls=%async_computation.6 | async-start | bytes 2097152 | tf_op jit(solution)/shard_map/psum | solution.py:46
  317.6 197.3 %all-reduce.7.cloned.1.call-start = ((), (), s32[]{:S(2)}) async-start(), calls=%async_computation.7 | async-start | bytes 4194304 | tf_op jit(solution)/shard_map/psum | solution.py:77
  430.6 84.3 %copy-start.3 = (f32[2048,256]{1,0:T(8,128)S(1)}, f32[2048,256]{1,0:T(8,128)}, u32[]{:S(2)}) copy-start(f32[2048,256]{1,0:T(8,128)} %param.15) | copy-start | bytes 6291460
  514.9 2.9 copy-start.4
  514.9 2.9 copy-start.6
  517.8 1.6 copy-start.7
Sparse Core Ops, SparseCore 0:
  10.1 123.0 all-gather.4
  135.2 123.1 all-gather.6
  265.6 85.6 all-gather.8
  353.9 72.2 all-gather.10
  428.9 20.7 all-reduce.4
  452.5 62.3 all-reduce.6
where the time goes:
time: 530 us; the launch traced here: 527 us
  waiting for transfers between devices  448 us (85%)
  matrix products  34.9 us (7%)
  between operations  14.2 us (3%)
  starting transfers between devices  12.9 us (2%)
  other arithmetic  10.6 us (2%)
  local copies, waits for them, and re-layouts  6.13 us (1%)
    all_gather x1, waiting for transfers between devices, body(): up_whole = lax.all_gather(up_weight, 'fs', axis=0, tiled=True)  123 us
    all_gather x1, waiting for transfers between devices, body(): down_whole = lax.all_gather(down_weight, 'fs', axis=1, tiled=True)  119 us
    all_gather x1, waiting for transfers between devices, body(): lax.all_gather(hidden_saved, 'fs', axis=0, tiled=True)  70.2 us
    psum x1, waiting for transfers between devices, body(): lax.psum(up_grad.astype(jnp.bfloat16), 'rep').astype(jnp.float32)  61.6 us
    all_gather x1, waiting for transfers between devices, body(): lax.all_gather(pre_grad, 'fs', axis=0, tiled=True)  31.9 us
    all_to_all x1, waiting for transfers between devices, body(): lax.all_to_all(cotangent, 'fs', split_axis=1, concat_axis=0, tiled=True)  21.9 us
    psum x1, waiting for transfers between devices, body(): lax.psum(mixed_part.astype(jnp.bfloat16), 'tp').astype(jnp.float32)  19.1 us
  transfers between devices with their start and end apart: 8, of which 8 were waited for; matrix products, arithmetic and copies ran while one was open for 7% of the time, Pallas kernels for 0%

commit v1 on v0

--- a/solution.py
+++ b/solution.py
@@ -80,9 +80,134 @@
     return (mixed, input_gradient_rows, up_sum + up_added, down_sum + down_added)
 
 
+def swap(values, axis):
+    size = lax.axis_size(axis)
+    return lax.ppermute(values, axis, [(i, i ^ 1) for i in range(size)])
+
+
+def own_half(values, axis_index, dim):
+    return lax.dynamic_index_in_dim(values, axis_index, dim, keepdims=False)
+
+
+def line_shift(values, shift):
+    size = lax.axis_size("fs")
+    outer = size // 2
+    return lax.ppermute(
+        values, "fs", [(i, ((i // 2 + shift) % outer) * 2 + i % 2) for i in range(size)]
+    )
+
+
+def ordered(first, second, axis_index):
+    return jnp.where(axis_index == 0, jnp.stack([first, second]), jnp.stack([second, first]))
+
+
+def gather_tokens(values):
+    rows, width = values.shape
+    outer = lax.axis_size("fs") // 2
+    half = own_half(values.reshape(2, rows // 2, width), lax.axis_index("tp"), 0)
+    line = jnp.stack([half] + [line_shift(half, s) for s in range(1, outer)])
+    both = jnp.stack([line, swap(line, "fs")])
+    return jnp.stack([both, swap(both, "tp")]).reshape(-1, width)
+
+
+def scatter_tokens(partial, rows):
+    width = partial.shape[1]
+    outer = lax.axis_size("fs") // 2
+    blocks = partial.reshape(2, 2, outer, rows // 2, width)
+    got = swap(blocks[1], "tp")
+    blocks = (blocks[0].astype(jnp.float32) + got.astype(jnp.float32)).astype(jnp.bfloat16)
+    got = swap(blocks[1], "fs")
+    blocks = (blocks[0].astype(jnp.float32) + got.astype(jnp.float32)).astype(jnp.bfloat16)
+    total = blocks[0].astype(jnp.float32)
+    for s in range(1, outer):
+        total = total + line_shift(blocks[s], -s).astype(jnp.float32)
+    half = total.astype(jnp.bfloat16)
+    whole = ordered(half, swap(half, "tp"), lax.axis_index("tp"))
+    return whole.reshape(rows, width).astype(jnp.float32)
+
+
+def hidden_body(
+    x_later, kept_input_rows, cotangent, norm_gain_vector, up_weight, down_weight, up_sum, down_sum
+):
+    row_count, width = x_later.shape
+    n_fs = lax.axis_size("fs")
+    grad_scale = float(row_count * lax.axis_size("rep") * n_fs) ** (-0.5)
+    group = lax.axis_index("rep")
+    depth, units = up_weight.shape
+    own_units = units // n_fs
+    inv_later, unit_later, normed_later = norm_partial_terms(x_later, norm_gain_vector)
+    inverse_rms_kept, unit_kept_rows, normed_kept_rows = norm_partial_terms(
+        kept_input_rows, norm_gain_vector
+    )
+    part = own_units // 2
+    up_half = own_half(up_weight.reshape(depth, n_fs, 2, part), group, 2)
+    down_half = own_half(down_weight.reshape(n_fs, 2, part, depth), group, 1)
+    up_half = lax.all_to_all(up_half.transpose(1, 0, 2), "fs", 0, 0, tiled=True)
+    down_half = lax.all_to_all(down_half, "fs", 0, 0, tiled=True)
+    up_half = up_half.reshape(width, part)
+    down_half = down_half.transpose(1, 0, 2).reshape(part, width)
+    up_own = jnp.concatenate([up_half, swap(up_half, "rep")], axis=1)
+    down_own = jnp.concatenate([down_half, swap(down_half, "rep")], axis=0)
+
+    normed_saved = gather_tokens(normed_kept_rows)
+    cot = gather_tokens(cotangent)
+    normed_next = gather_tokens(normed_later)
+
+    pre_saved = jnp.dot(normed_saved, up_own, preferred_element_type=jnp.float32)
+    hidden_saved = squared_relu(pre_saved)
+    hidden_grad = lax.dot_general(cot, down_own, TRANSPOSED, preferred_element_type=jnp.float32)
+    pre_grad = (hidden_grad * 2.0 * jax.nn.relu(pre_saved)).astype(jnp.bfloat16)
+    up_grad = grad_scale * lax.dot_general(
+        normed_saved, pre_grad, LEADING, preferred_element_type=jnp.float32
+    )
+    down_grad = grad_scale * lax.dot_general(
+        hidden_saved, cot, LEADING, preferred_element_type=jnp.float32
+    )
+    up_got = swap(up_grad[:, part:].astype(jnp.bfloat16), "rep")
+    down_got = swap(down_grad[part:].astype(jnp.bfloat16), "rep")
+    back_part = lax.dot_general(pre_grad, up_own, TRANSPOSED, preferred_element_type=jnp.float32)
+    hidden_later = squared_relu(
+        jnp.dot(normed_next, up_own, preferred_element_type=jnp.float32)
+    )
+    mixed_part = jnp.dot(hidden_later, down_own, preferred_element_type=jnp.float32)
+    up_half = (up_grad[:, :part] + up_got.astype(jnp.float32)).astype(jnp.bfloat16)
+    down_half = (down_grad[:part] + down_got.astype(jnp.float32)).astype(jnp.bfloat16)
+    up_half = lax.all_to_all(up_half.reshape(n_fs, depth, part), "fs", 0, 0, tiled=True)
+    down_half = down_half.reshape(part, n_fs, depth).transpose(1, 0, 2)
+    down_half = lax.all_to_all(down_half, "fs", 0, 0, tiled=True)
+    up_added = ordered(up_half, swap(up_half, "rep"), group)
+    up_added = up_added.transpose(2, 1, 0, 3).reshape(depth, units)
+    down_added = ordered(down_half, swap(down_half, "rep"), group)
+    down_added = down_added.transpose(1, 0, 2, 3).reshape(units, depth)
+
+    back_sum = scatter_tokens(back_part.astype(jnp.bfloat16), row_count)
+    mixed = scatter_tokens(mixed_part.astype(jnp.bfloat16), row_count).astype(jnp.bfloat16)
+    scaled_rows = back_sum * norm_gain_vector
+    input_gradient_rows = (
+        inverse_rms_kept
+        * (
+            scaled_rows
+            - unit_kept_rows * jnp.mean(scaled_rows * unit_kept_rows, axis=-1, keepdims=True)
+        )
+    ).astype(jnp.bfloat16)
+    return (
+        mixed,
+        input_gradient_rows,
+        up_sum + up_added.astype(jnp.float32),
+        down_sum + down_added.astype(jnp.float32),
+    )
+
+
+def chosen_body(*args):
+    units = args[4].shape[1]
+    n_fs = lax.axis_size("fs")
+    pairs = lax.axis_size("tp") == 2 and lax.axis_size("rep") == 2 and n_fs % 2 == 0
+    return (hidden_body if pairs and units % (128 * n_fs) == 0 else body)(*args)
+
+
 def solution(mesh):
     return jax.shard_map(
-        body,
+        chosen_body,
         mesh=mesh,
         in_specs=(
             P(("rep", "fs"), None),

time: 530 us -> 363 us (0.68)
  waiting for transfers between devices: 448 us -> 200 us
  starting transfers between devices: 12.9 us -> 79.7 us
  other arithmetic: 10.6 us -> 39.5 us
  matrix products: 34.9 us -> 16.4 us
  local copies, waits for them, and re-layouts: 6.13 us -> 22.2 us
  between operations: 14.2 us -> 1.07 us
    all_gather x4 -> x0, waiting for transfers between devices: 344 us -> none  [the longest x1 123 us: body(): up_whole = lax.all_gather(up_weight, 'fs', axis=0, tiled=True)]
    ppermute x0 -> x33, waiting for transfers between devices: none -> 175 us  [the longest x18 87.5 us: swap(): return lax.ppermute(values, axis, [(i, i ^ 1) for i in range(size)])]
    psum x2 -> x0, waiting for transfers between devices: 80.7 us -> none  [the longest x1 61.6 us: body(): lax.psum(up_grad.astype(jnp.bfloat16), 'rep').astype(jnp.float32)]
    ppermute x0 -> x33, starting transfers between devices: none -> 55.5 us  [the longest x18 30.2 us: swap(): return lax.ppermute(values, axis, [(i, i ^ 1) for i in range(size)])]
    dot_general x6, matrix products: 34.9 us -> 16.4 us  [the longest x1 8.74 us: hidden_body(): jnp.dot(hidden_later, down_own, preferred_element_type=jnp.float32)]
    another operation x0 -> x9, other arithmetic: none -> 18 us  [the longest x6 15.2 us: gather_tokens(): return jnp.stack([both, swap(both, 'tp')]).reshape(-1, width)]
    all_to_all x2 -> x4, starting transfers between devices: 12.5 us -> 24.2 us  [the longest x2 11.4 us: hidden_body(): down_half = lax.all_to_all(down_half, 'fs', 0, 0, tiled=True)]
    convert_element_type x2 -> x11, other arithmetic: 3.1 us -> 10.6 us  [the longest x4 3.56 us: scatter_tokens(): (blocks[0].astype(jnp.float32) + got.astype(jnp.float32)).astype(jnp.bflo...]
  transfers between devices with their start and end apart: 8 -> 37, of which waited for: 8 -> 26; matrix products, arithmetic and copies ran while one was open for 7% -> 14% of each run, Pallas kernels for 0% -> 0%
where the time goes in v1:
time: 363 us; the launch traced here: 358 us
  waiting for transfers between devices  200 us (55%)
  starting transfers between devices  79.7 us (22%)
  other arithmetic  39.5 us (11%)
  local copies, waits for them, and re-layouts  22.2 us (6%)
  matrix products  16.4 us (5%)
    ppermute x18, waiting for transfers between devices, swap(): return lax.ppermute(values, axis, [(i, i ^ 1) for i in range(size)])  87.5 us
    ppermute x15, waiting for transfers between devices, line_shift(): lax.ppermute(values, 'fs', [(i, (i // 2 + shift) % outer * 2 + i % 2) for...  87.2 us
    ppermute x18, starting transfers between devices, swap(): return lax.ppermute(values, axis, [(i, i ^ 1) for i in range(size)])  30.2 us
    ppermute x15, starting transfers between devices, line_shift(): lax.ppermute(values, 'fs', [(i, (i // 2 + shift) % outer * 2 + i % 2) for...  25.3 us
    another operation x6, other arithmetic, gather_tokens(): return jnp.stack([both, swap(both, 'tp')]).reshape(-1, width)  15.2 us
    all_to_all x1, waiting for transfers between devices, hidden_body(): up_half = lax.all_to_all(up_half.transpose(1, 0, 2), 'fs', 0, 0, tiled=True)  11.5 us
    all_to_all x2, starting transfers between devices, hidden_body(): down_half = lax.all_to_all(down_half, 'fs', 0, 0, tiled=True)  11.4 us
    dot_general x1, matrix products, hidden_body(): jnp.dot(hidden_later, down_own, preferred_element_type=jnp.float32)  8.74 us
  transfers between devices with their start and end apart: 37, of which 26 were waited for; matrix products, arithmetic and copies ran while one was open for 14% of the time, Pallas kernels for 0%

profile of v1, /device:TPU:11, one launch (start us, length us, event | category | flops | bytes accessed | tf_op | source)
XLA Modules:
  0.0 358.4 jit_solution(4641211509036308654)
XLA Ops:
  2.0 2.3 collective-permute-start.14
  4.3 2.2 collective-permute-start.13
  10.3 2.1 collective-permute-start.18
  12.4 8.5 %collective-permute-done.14 = bf16[64,2048]{1,0:T(8,128)(2,1)S(1)} collective-permute-done((bf16[64,2048]{1,0:T(8,128)(2,1)S(1)}, bf16[64,2048]{1,0:T(8,128)(2,1)S(1)}, u32[]{:S(2)}, u32[]{:S(2)}) %collective-permute-start.14) | collective-permute-done | bytes 262176 | tf_op jit(solution)/shard_map/ppermute | solution.py:95
  20.9 16.9 %collective-permute-done.13 = bf16[64,2048]{1,0:T(8,128)(2,1)S(1)} collective-permute-done((bf16[64,2048]{1,0:T(8,128)(2,1)S(1)}, bf16[64,2048]{1,0:T(8,128)(2,1)S(1)}, u32[]{:S(2)}, u32[]{:S(2)}) %collective-permute-start.13) | collective-permute-done | bytes 262176 | tf_op jit(solution)/shard_map/ppermute | solution.py:95
  40.2 2.5 collective-permute-done.20
  43.4 5.6 %collective-permute-done.18 = bf16[64,2048]{1,0:T(8,128)(2,1)S(1)} collective-permute-done((bf16[64,2048]{1,0:T(8,128)(2,1)S(1)}, bf16[64,2048]{1,0:T(8,128)(2,1)S(1)}, u32[]{:S(2)}, u32[]{:S(2)}) %collective-permute-start.18) | collective-permute-done | bytes 262176 | tf_op jit(solution)/shard_map/ppermute | solution.py:95
  49.0 1.5 fusion.39
  51.8 9.8 %collective-permute-done.16 = bf16[4,64,2048]{2,1,0:T(8,128)(2,1)S(1)} collective-permute-done((bf16[4,64,2048]{2,1,0:T(8,128)(2,1)S(1)}, bf16[4,64,2048]{2,1,0:T(8,128)(2,1)S(1)}, u32[]{:S(2)}, u32[]{:S(2)}) %collective-permute-start.16) | collective-permute-done | bytes 1048608 | tf_op jit(solution)/shard_map/ppermute | solution.py:85
  62.5 3.2 fusion.37
  65.7 5.4 %collective-permute-start.17 = (bf16[2,4,64,2048]{3,2,1,0:T(8,128)(2,1)}, bf16[2,4,64,2048]{3,2,1,0:T(8,128)(2,1)}, u32[]{:S(2)}, u32[]{:S(2)}) collective-permute-start(bf16[2,4,64,2048]{3,2,1,0:T(8,128)(2,1)} %get-tuple-element.9), channel_id=1, source_target_pairs={{0,1},{1,0},{2,3},{3,2},{4,5},{5,4},{6,7},{7,6},{8,9},{9,8},{10,11... | collective-permute-start | bytes 6291464 | tf_op jit(solution)/shard_map/ppermute | solution.py:85
  72.0 2.0 copy.37
  74.0 5.6 %all-to-all-start.1 = ((bf16[8,128,256]{1,2,0:T(8,128)(2,1)}), bf16[8,128,256]{1,2,0:T(8,128)(2,1)}, u32[]{:S(2)}, u32[]{:S(2)}) async-start(bf16[8,128,256]{1,2,0:T(8,128)(2,1)} %bitcast.16), calls=%async_computation.1 | async-start | bytes 1048576 | tf_op jit(solution)/shard_map/all_to_all | solution.py:146
  79.6 6.4 %collective-permute-done.21 = bf16[4,64,2048]{2,1,0:T(8,128)(2,1)} collective-permute-done((bf16[4,64,2048]{2,1,0:T(8,128)(2,1)}, bf16[4,64,2048]{2,1,0:T(8,128)(2,1)}, u32[]{:S(2)}, u32[]{:S(2)}) %collective-permute-start.21) | collective-permute-done | bytes 1048608 | tf_op jit(solution)/shard_map/ppermute | solution.py:85
  86.0 3.8 %fusion.36 = (bf16[1,2,4,64,2048]{4,3,2,1,0:T(8,128)(2,1)}, bf16[2,4,64,2048]{3,2,1,0:T(8,128)(2,1)}) fusion(bf16[1,4,64,2048]{3,2,1,0:T(8,128)(2,1)} %bitcast.47, bf16[1,4,64,2048]{3,2,1,0:T(8,128)(2,1)} %get-tuple-element.19), kind=kLoop, calls=%fused_computation.96 | loop fusion | flops 1048576 | bytes 6291456 | tf_op jit(solution)/shard_map/stack | solution.py:110
  89.8 5.3 %collective-permute-start.22 = (bf16[2,4,64,2048]{3,2,1,0:T(8,128)(2,1)}, bf16[2,4,64,2048]{3,2,1,0:T(8,128)(2,1)}, u32[]{:S(2)}, u32[]{:S(2)}) collective-permute-start(bf16[2,4,64,2048]{3,2,1,0:T(8,128)(2,1)} %get-tuple-element.11), channel_id=1, source_target_pairs={{0,1},{1,0},{2,3},{3,2},{4,5},{5,4},{6,7},{7,6},{8,9},{9,8},{10,11... | collective-permute-start | bytes 6291464 | tf_op jit(solution)/shard_map/ppermute | solution.py:85
  95.2 1.5 copy.30
  97.5 2.0 copy.32
  99.5 6.2 %all-to-all-start = ((bf16[8,256,128]{2,1,0:T(8,128)(2,1)}), bf16[8,256,128]{2,1,0:T(8,128)(2,1)S(1)}, u32[]{:S(2)}, u32[]{:S(2)}) async-start(bf16[8,256,128]{2,1,0:T(8,128)(2,1)} %copy.32), calls=%async_computation | async-start | bytes 1048576 | tf_op jit(solution)/shard_map/all_to_all | solution.py:145
  106.0 11.5 %all-to-all-done = bf16[8,256,128]{2,1,0:T(8,128)(2,1)S(1)} async-done(((bf16[8,256,128]{2,1,0:T(8,128)(2,1)}), bf16[8,256,128]{2,1,0:T(8,128)(2,1)S(1)}, u32[]{:S(2)}, u32[]{:S(2)}) %all-to-all-start) | async-done | bytes 524320 | tf_op jit(solution)/shard_map/all_to_all | solution.py:145
  117.7 2.1 pad_maximum_fusion.1
  120.0 3.4 pad_maximum_fusion.2
  123.4 4.8 %collective-permute-done.5 = bf16[2048,128]{1,0:T(8,128)(2,1)S(1)} collective-permute-done((bf16[2048,128]{1,0:T(8,128)(2,1)S(1)}, bf16[2048,128]{1,0:T(8,128)(2,1)S(1)}, u32[]{:S(2)}, u32[]{:S(2)}) %collective-permute-start.5) | collective-permute-done | bytes 524320 | tf_op jit(solution)/shard_map/ppermute | solution.py:85
  129.5 2.5 fusion.9
  133.9 3.7 %collective-permute-start.23 = (bf16[2,4,64,2048]{3,2,1,0:T(8,128)(2,1)S(1)}, bf16[2,4,64,2048]{3,2,1,0:T(8,128)(2,1)S(1)}, u32[]{:S(2)}, u32[]{:S(2)}) collective-permute-start(bf16[2,4,64,2048]{3,2,1,0:T(8,128)(2,1)S(1)} %bitcast.145), channel_id=1, source_target_pairs={{0,1},{1,0},{2,3},{3,2},{4,5},{5,4},{6,7},{7,6},{8,9},{9,8},{10,11... | collective-permute-start | bytes 6291464 | tf_op jit(solution)/shard_map/ppermute | solution.py:85
  137.5 3.8 %collective-permute-done.23 = bf16[2,4,64,2048]{3,2,1,0:T(8,128)(2,1)S(1)} collective-permute-done((bf16[2,4,64,2048]{3,2,1,0:T(8,128)(2,1)S(1)}, bf16[2,4,64,2048]{3,2,1,0:T(8,128)(2,1)S(1)}, u32[]{:S(2)}, u32[]{:S(2)}) %collective-permute-start.23) | collective-permute-done | bytes 2097184 | tf_op jit(solution)/shard_map/ppermute | solution.py:85
  142.2 1.5 collective-permute-start.24
  143.8 22.9 %collective-permute-done.24 = bf16[4,64,2048]{2,1,0:T(8,128)(2,1)S(1)} collective-permute-done((bf16[4,64,2048]{2,1,0:T(8,128)(2,1)S(1)}, bf16[4,64,2048]{2,1,0:T(8,128)(2,1)S(1)}, u32[]{:S(2)}, u32[]{:S(2)}) %collective-permute-start.24) | collective-permute-done | bytes 1048608 | tf_op jit(solution)/shard_map/ppermute | solution.py:85
  167.1 2.4 collective-permute-start.25
  169.5 3.9 %collective-permute-start.26 = (bf16[64,2048]{1,0:T(8,128)(2,1)S(1)}, bf16[64,2048]{1,0:T(8,128)(2,1)S(1)}, u32[]{:S(2)}, u32[]{:S(2)}) collective-permute-start(bf16[64,2048]{1,0:T(8,128)(2,1)S(1)} %get-tuple-element.16), channel_id=1, source_target_pairs={{0,8},{2,10},{4,12},{6,14},{8,0},{10,2},{12,4},{14,6},{1,9},{3,11}... | collective-permute-start | bytes 786440 | tf_op jit(solution)/shard_map/ppermute | solution.py:95
  174.5 7.7 %collective-permute-done.27 = bf16[64,2048]{1,0:T(8,128)(2,1)S(1)} collective-permute-done((bf16[64,2048]{1,0:T(8,128)(2,1)S(1)}, bf16[64,2048]{1,0:T(8,128)(2,1)S(1)}, u32[]{:S(2)}, u32[]{:S(2)}) %collective-permute-start.27) | collective-permute-done | bytes 262176 | tf_op jit(solution)/shard_map/ppermute | solution.py:95
  182.2 8.6 %collective-permute-done.26 = bf16[64,2048]{1,0:T(8,128)(2,1)S(1)} collective-permute-done((bf16[64,2048]{1,0:T(8,128)(2,1)S(1)}, bf16[64,2048]{1,0:T(8,128)(2,1)S(1)}, u32[]{:S(2)}, u32[]{:S(2)}) %collective-permute-start.26) | collective-permute-done | bytes 262176 | tf_op jit(solution)/shard_map/ppermute | solution.py:95
  191.0 2.1 collective-permute-start.28
  197.6 1.5 collective-permute-start.2
  199.1 1.7 collective-permute-start.1
  200.8 2.3 collective-permute-start
  203.1 2.0 collective-permute-done.2
  205.1 12.3 %collective-permute-done.1 = bf16[64,2048]{1,0:T(8,128)(2,1)S(1)} collective-permute-done((bf16[64,2048]{1,0:T(8,128)(2,1)S(1)}, bf16[64,2048]{1,0:T(8,128)(2,1)S(1)}, u32[]{:S(2)}, u32[]{:S(2)}) %collective-permute-start.1) | collective-permute-done | bytes 262176 | tf_op jit(solution)/shard_map/ppermute | solution.py:95
  217.4 5.6 %collective-permute-done = bf16[64,2048]{1,0:T(8,128)(2,1)S(1)} collective-permute-done((bf16[64,2048]{1,0:T(8,128)(2,1)S(1)}, bf16[64,2048]{1,0:T(8,128)(2,1)S(1)}, u32[]{:S(2)}, u32[]{:S(2)}) %collective-permute-start) | collective-permute-done | bytes 262176 | tf_op jit(solution)/shard_map/ppermute | solution.py:95
  223.2 1.5 collective-permute-start.3
  224.7 22.1 %collective-permute-done.3 = bf16[4,64,2048]{2,1,0:T(8,128)(2,1)S(1)} collective-permute-done((bf16[4,64,2048]{2,1,0:T(8,128)(2,1)S(1)}, bf16[4,64,2048]{2,1,0:T(8,128)(2,1)S(1)}, u32[]{:S(2)}, u32[]{:S(2)}) %collective-permute-start.3) | collective-permute-done | bytes 1048608 | tf_op jit(solution)/shard_map/ppermute | solution.py:85
  247.0 2.1 collective-permute-start.4
  249.2 3.8 %collective-permute-done.4 = bf16[2,4,64,2048]{3,2,1,0:T(8,128)(2,1)S(1)} collective-permute-done((bf16[2,4,64,2048]{3,2,1,0:T(8,128)(2,1)S(1)}, bf16[2,4,64,2048]{3,2,1,0:T(8,128)(2,1)S(1)}, u32[]{:S(2)}, u32[]{:S(2)}) %collective-permute-start.4) | collective-permute-done | bytes 2097184 | tf_op jit(solution)/shard_map/ppermute | solution.py:85
  253.0 2.4 pad_maximum_fusion
  255.4 8.7 %convolution_convert_fusion.1 = bf16[1024,2048]{1,0:T(8,128)(2,1)} fusion(bf16[1024,2048]{1,0:T(8,128)(2,1)} %bitcast.133, bf16[128,2048]{0,1:T(8,128)(2,1)} %collective-permute-done.6, bf16[128,2048]{0,1:T(8,128)(2,1)} %bitcast.18, bf16[2048,128]{1,0:T(8,128)(2,1)S(1)} %copy-done.15, bf16[2048,128]{1,0:T(8,128)(2,1)S(1)} %bitcast.138), kind=kOutput, calls=%fused_computation.8 | convolution fusion | flops 2154561536 | bytes 10485760 | tf_op jit(solution)/shard_map/dot_general | solution.py:172
  264.2 2.9 fusion.43
  275.6 8.5 %collective-permute-done.31 = bf16[128,2048]{1,0:T(8,128)(2,1)S(1)} collective-permute-done((bf16[128,2048]{1,0:T(8,128)(2,1)S(1)}, bf16[128,2048]{1,0:T(8,128)(2,1)S(1)}, u32[]{:S(2)}, u32[]{:S(2)}) %collective-permute-start.31) | collective-permute-done | bytes 524320 | tf_op jit(solution)/shard_map/ppermute | solution.py:85
  285.0 5.8 %all-to-all-start.3 = ((bf16[8,128,256]{2,1,0:T(8,128)(2,1)}), bf16[8,128,256]{2,1,0:T(8,128)(2,1)}, u32[]{:S(2)}, u32[]{:S(2)}) async-start(bf16[8,128,256]{2,1,0:T(8,128)(2,1)} %bitcast.125), calls=%async_computation.3 | async-start | bytes 1048576 | tf_op jit(solution)/shard_map/all_to_all | solution.py:177
  290.8 4.5 %collective-permute-done.29 = bf16[2048,128]{1,0:T(8,128)(2,1)} collective-permute-done((bf16[2048,128]{1,0:T(8,128)(2,1)S(1)}, bf16[2048,128]{1,0:T(8,128)(2,1)}, u32[]{:S(2)}, u32[]{:S(2)}) %collective-permute-start.29) | collective-permute-done | bytes 524320 | tf_op jit(solution)/shard_map/ppermute | solution.py:85
  295.3 2.3 fusion.21
  297.5 5.6 %all-to-all-done.3 = bf16[8,128,256]{2,1,0:T(8,128)(2,1)} async-done(((bf16[8,128,256]{2,1,0:T(8,128)(2,1)}), bf16[8,128,256]{2,1,0:T(8,128)(2,1)}, u32[]{:S(2)}, u32[]{:S(2)}) %all-to-all-start.3) | async-done | bytes 524320 | tf_op jit(solution)/shard_map/all_to_all | solution.py:177
  303.1 6.5 %all-to-all-start.2 = ((bf16[8,256,128]{2,1,0:T(8,128)(2,1)}), bf16[8,256,128]{2,1,0:T(8,128)(2,1)}, u32[]{:S(2)}, u32[]{:S(2)}) async-start(bf16[8,256,128]{2,1,0:T(8,128)(2,1)} %bitcast.62), calls=%async_computation.2 | async-start | bytes 1048576 | tf_op jit(solution)/shard_map/all_to_all | solution.py:175
  309.9 1.6 fusion.3
  313.1 3.9 %collective-permute-start.10 = (bf16[64,2048]{1,0:T(8,128)(2,1)S(1)}, bf16[64,2048]{1,0:T(8,128)(2,1)S(1)}, u32[]{:S(2)}, u32[]{:S(2)}) collective-permute-start(bf16[64,2048]{1,0:T(8,128)(2,1)S(1)} %get-tuple-element.23), channel_id=1, source_target_pairs={{0,8},{2,10},{4,12},{6,14},{8,0},{10,2},{12,4},{14,6},{1,9},{3,11}... | collective-permute-start | bytes 786440 | tf_op jit(solution)/shard_map/ppermute | solution.py:95
  317.0 7.9 %all-to-all-done.2 = bf16[8,256,128]{2,1,0:T(8,128)(2,1)} async-done(((bf16[8,256,128]{2,1,0:T(8,128)(2,1)}), bf16[8,256,128]{2,1,0:T(8,128)(2,1)}, u32[]{:S(2)}, u32[]{:S(2)}) %all-to-all-start.2) | async-done | bytes 524320 | tf_op jit(solution)/shard_map/all_to_all | solution.py:175
  325.1 1.9 fusion.22
  327.0 11.7 %collective-permute-done.9 = bf16[64,2048]{1,0:T(8,128)(2,1)S(1)} collective-permute-done((bf16[64,2048]{1,0:T(8,128)(2,1)S(1)}, bf16[64,2048]{1,0:T(8,128)(2,1)S(1)}, u32[]{:S(2)}, u32[]{:S(2)}) %collective-permute-start.9) | collective-permute-done | bytes 262176 | tf_op jit(solution)/shard_map/ppermute | solution.py:95
  338.6 4.0 %collective-permute-done.10 = bf16[64,2048]{1,0:T(8,128)(2,1)S(1)} collective-permute-done((bf16[64,2048]{1,0:T(8,128)(2,1)S(1)}, bf16[64,2048]{1,0:T(8,128)(2,1)S(1)}, u32[]{:S(2)}, u32[]{:S(2)}) %collective-permute-start.10) | collective-permute-done | bytes 262176 | tf_op jit(solution)/shard_map/ppermute | solution.py:95
  342.8 1.6 collective-permute-start.12
  344.4 1.6 bitcast_add_fusion
  347.4 2.9 copy.34
  350.3 2.9 reshape.124
  353.3 3.2 add.85
  356.5 1.9 maximum_select_fusion.2
  (107 shorter events, 36.3 us)
Async XLA Ops:
  0.6 70.5 %copy-start = (bf16[2048,256]{1,0:T(8,128)(2,1)S(1)}, bf16[2048,256]{1,0:T(8,128)(2,1)}, u32[]{:S(2)}) copy-start(bf16[2048,256]{1,0:T(8,128)(2,1)} %param.13) | copy-start | bytes 3145732
  0.6 9.6 %copy-start.16 = (bf16[128,2048]{1,0:T(8,128)(2,1)S(1)}, bf16[128,2048]{1,0:T(8,128)(2,1)}, u32[]{:S(2)}) copy-start(bf16[128,2048]{1,0:T(8,128)(2,1)} %param.10) | copy-start | bytes 1572868
  1.8 8.5 %collective-permute-start.15 = (bf16[64,2048]{1,0:T(8,128)(2,1)S(1)}, bf16[64,2048]{1,0:T(8,128)(2,1)S(1)}, u32[]{:S(2)}, u32[]{:S(2)}) collective-permute-start(bf16[64,2048]{1,0:T(8,128)(2,1)S(1)} %fusion.52), channel_id=1, source_target_pairs={{0,12},{2,14},{4,0},{6,2},{8,4},{10,6},{12,8},{14,10},{1,13},{3,15... | collective-permute-start | bytes 786440 | tf_op jit(solution)/shard_map/ppermute | solution.py:95
  2.0 18.9 %collective-permute-start.14 = (bf16[64,2048]{1,0:T(8,128)(2,1)S(1)}, bf16[64,2048]{1,0:T(8,128)(2,1)S(1)}, u32[]{:S(2)}, u32[]{:S(2)}) collective-permute-start(bf16[64,2048]{1,0:T(8,128)(2,1)S(1)} %fusion.52), channel_id=1, source_target_pairs={{0,8},{2,10},{4,12},{6,14},{8,0},{10,2},{12,4},{14,6},{1,9},{3,11}... | collective-permute-start | bytes 786440 | tf_op jit(solution)/shard_map/ppermute | solution.py:95
  4.3 33.5 %collective-permute-start.13 = (bf16[64,2048]{1,0:T(8,128)(2,1)S(1)}, bf16[64,2048]{1,0:T(8,128)(2,1)S(1)}, u32[]{:S(2)}, u32[]{:S(2)}) collective-permute-start(bf16[64,2048]{1,0:T(8,128)(2,1)S(1)} %fusion.52), channel_id=1, source_target_pairs={{0,4},{2,6},{4,8},{6,10},{8,12},{10,14},{12,0},{14,2},{1,5},{3,7},... | collective-permute-start | bytes 786440 | tf_op jit(solution)/shard_map/ppermute | solution.py:95
  9.0 33.7 %collective-permute-start.20 = (bf16[64,2048]{1,0:T(8,128)(2,1)S(1)}, bf16[64,2048]{1,0:T(8,128)(2,1)S(1)}, u32[]{:S(2)}, u32[]{:S(2)}) collective-permute-start(bf16[64,2048]{1,0:T(8,128)(2,1)S(1)} %fusion.53), channel_id=1, source_target_pairs={{0,12},{2,14},{4,0},{6,2},{8,4},{10,6},{12,8},{14,10},{1,13},{3,15... | collective-permute-start | bytes 786440 | tf_op jit(solution)/shard_map/ppermute | solution.py:95
  9.1 34.3 %collective-permute-start.19 = (bf16[64,2048]{1,0:T(8,128)(2,1)S(1)}, bf16[64,2048]{1,0:T(8,128)(2,1)S(1)}, u32[]{:S(2)}, u32[]{:S(2)}) collective-permute-start(bf16[64,2048]{1,0:T(8,128)(2,1)S(1)} %fusion.53), channel_id=1, source_target_pairs={{0,8},{2,10},{4,12},{6,14},{8,0},{10,2},{12,4},{14,6},{1,9},{3,11}... | collective-permute-start | bytes 786440 | tf_op jit(solution)/shard_map/ppermute | solution.py:95
  10.3 38.7 %collective-permute-start.18 = (bf16[64,2048]{1,0:T(8,128)(2,1)S(1)}, bf16[64,2048]{1,0:T(8,128)(2,1)S(1)}, u32[]{:S(2)}, u32[]{:S(2)}) collective-permute-start(bf16[64,2048]{1,0:T(8,128)(2,1)S(1)} %fusion.53), channel_id=1, source_target_pairs={{0,4},{2,6},{4,8},{6,10},{8,12},{10,14},{12,0},{14,2},{1,5},{3,7},... | collective-permute-start | bytes 786440 | tf_op jit(solution)/shard_map/ppermute | solution.py:95
  38.9 22.7 %collective-permute-start.16 = (bf16[4,64,2048]{2,1,0:T(8,128)(2,1)S(1)}, bf16[4,64,2048]{2,1,0:T(8,128)(2,1)S(1)}, u32[]{:S(2)}, u32[]{:S(2)}) collective-permute-start(bf16[4,64,2048]{2,1,0:T(8,128)(2,1)S(1)} %get-tuple-element.18), channel_id=1, source_target_pairs={{0,2},{2,0},{4,6},{6,4},{8,10},{10,8},{12,14},{14,12},{1,3},{3,1},... | collective-permute-start | bytes 3145736 | tf_op jit(solution)/shard_map/ppermute | solution.py:85
  50.5 35.5 %collective-permute-start.21 = (bf16[4,64,2048]{2,1,0:T(8,128)(2,1)}, bf16[4,64,2048]{2,1,0:T(8,128)(2,1)}, u32[]{:S(2)}, u32[]{:S(2)}) collective-permute-start(bf16[4,64,2048]{2,1,0:T(8,128)(2,1)} %get-tuple-element.20), channel_id=1, source_target_pairs={{0,2},{2,0},{4,6},{6,4},{8,10},{10,8},{12,14},{14,12},{1,3},{3,1},... | collective-permute-start | bytes 3145736 | tf_op jit(solution)/shard_map/ppermute | solution.py:85
  61.6 1.0 copy-start.13
  65.7 52.0 %collective-permute-start.17 = (bf16[2,4,64,2048]{3,2,1,0:T(8,128)(2,1)}, bf16[2,4,64,2048]{3,2,1,0:T(8,128)(2,1)}, u32[]{:S(2)}, u32[]{:S(2)}) collective-permute-start(bf16[2,4,64,2048]{3,2,1,0:T(8,128)(2,1)} %get-tuple-element.9), channel_id=1, source_target_pairs={{0,1},{1,0},{2,3},{3,2},{4,5},{5,4},{6,7},{7,6},{8,9},{9,8},{10,11... | collective-permute-start | bytes 6291464 | tf_op jit(solution)/shard_map/ppermute | solution.py:85
  74.0 25.5 %all-to-all-start.1 = ((bf16[8,128,256]{1,2,0:T(8,128)(2,1)}), bf16[8,128,256]{1,2,0:T(8,128)(2,1)}, u32[]{:S(2)}, u32[]{:S(2)}) async-start(bf16[8,128,256]{1,2,0:T(8,128)(2,1)} %bitcast.16), calls=%async_computation.1 | async-start | bytes 1048576 | tf_op jit(solution)/shard_map/all_to_all | solution.py:146
  89.8 30.1 %collective-permute-start.22 = (bf16[2,4,64,2048]{3,2,1,0:T(8,128)(2,1)}, bf16[2,4,64,2048]{3,2,1,0:T(8,128)(2,1)}, u32[]{:S(2)}, u32[]{:S(2)}) collective-permute-start(bf16[2,4,64,2048]{3,2,1,0:T(8,128)(2,1)} %get-tuple-element.11), channel_id=1, source_target_pairs={{0,1},{1,0},{2,3},{3,2},{4,5},{5,4},{6,7},{7,6},{8,9},{9,8},{10,11... | collective-permute-start | bytes 6291464 | tf_op jit(solution)/shard_map/ppermute | solution.py:85
  99.5 17.9 %all-to-all-start = ((bf16[8,256,128]{2,1,0:T(8,128)(2,1)}), bf16[8,256,128]{2,1,0:T(8,128)(2,1)S(1)}, u32[]{:S(2)}, u32[]{:S(2)}) async-start(bf16[8,256,128]{2,1,0:T(8,128)(2,1)} %copy.32), calls=%async_computation | async-start | bytes 1048576 | tf_op jit(solution)/shard_map/all_to_all | solution.py:145
  105.8 23.7 %collective-permute-start.6 = (bf16[128,2048]{0,1:T(8,128)(2,1)}, bf16[128,2048]{0,1:T(8,128)(2,1)}, u32[]{:S(2)}, u32[]{:S(2)}) collective-permute-start(bf16[128,2048]{0,1:T(8,128)(2,1)} %bitcast.18), channel_id=1, source_target_pairs={{0,16},{16,0},{1,17},{17,1},{2,18},{18,2},{3,19},{19,3},{4,20},{20... | collective-permute-start | bytes 1572872 | tf_op jit(solution)/shard_map/ppermute | solution.py:85
  117.5 14.5 %copy-start.9 = (bf16[8,256,128]{2,1,0:T(8,128)(2,1)}, bf16[8,256,128]{2,1,0:T(8,128)(2,1)S(1)}, u32[]{:S(2)}) copy-start(bf16[8,256,128]{2,1,0:T(8,128)(2,1)S(1)} %all-to-all-done) | copy-start | bytes 1572868
  117.5 10.7 %collective-permute-start.5 = (bf16[2048,128]{1,0:T(8,128)(2,1)S(1)}, bf16[2048,128]{1,0:T(8,128)(2,1)S(1)}, u32[]{:S(2)}, u32[]{:S(2)}) collective-permute-start(bf16[2048,128]{1,0:T(8,128)(2,1)S(1)} %bitcast.135), channel_id=1, source_target_pairs={{0,16},{16,0},{1,17},{17,1},{2,18},{18,2},{3,19},{19,3},{4,20},{20... | collective-permute-start | bytes 1572872 | tf_op jit(solution)/shard_map/ppermute | solution.py:85
  117.7 2.2 copy-start.4
  119.9 9.6 %copy-start.2 = (bf16[2,2,4,64,2048]{4,3,2,1,0:T(8,128)(2,1)}, bf16[2,2,4,64,2048]{4,3,2,1,0:T(8,128)(2,1)S(1)}, u32[]{:S(2)}) copy-start(bf16[2,2,4,64,2048]{4,3,2,1,0:T(8,128)(2,1)S(1)} %pad_maximum_fusion.1) | copy-start | bytes 12582916
  123.4 6.1 %copy-start.6 = (bf16[2,2,4,64,2048]{4,3,2,1,0:T(8,128)(2,1)}, bf16[2,2,4,64,2048]{4,3,2,1,0:T(8,128)(2,1)S(1)}, u32[]{:S(2)}) copy-start(bf16[2,2,4,64,2048]{4,3,2,1,0:T(8,128)(2,1)S(1)} %pad_maximum_fusion.2) | copy-start | bytes 12582916
  128.2 3.8 %copy-start.14 = (bf16[2048,128]{1,0:T(8,128)(2,1)}, bf16[2048,128]{1,0:T(8,128)(2,1)S(1)}, u32[]{:S(2)}) copy-start(bf16[2048,128]{1,0:T(8,128)(2,1)S(1)} %collective-permute-done.5) | copy-start | bytes 1572868
  133.9 7.5 %collective-permute-start.23 = (bf16[2,4,64,2048]{3,2,1,0:T(8,128)(2,1)S(1)}, bf16[2,4,64,2048]{3,2,1,0:T(8,128)(2,1)S(1)}, u32[]{:S(2)}, u32[]{:S(2)}) collective-permute-start(bf16[2,4,64,2048]{3,2,1,0:T(8,128)(2,1)S(1)} %bitcast.145), channel_id=1, source_target_pairs={{0,1},{1,0},{2,3},{3,2},{4,5},{5,4},{6,7},{7,6},{8,9},{9,8},{10,11... | collective-permute-start | bytes 6291464 | tf_op jit(solution)/shard_map/ppermute | solution.py:85
  142.2 24.4 %collective-permute-start.24 = (bf16[4,64,2048]{2,1,0:T(8,128)(2,1)S(1)}, bf16[4,64,2048]{2,1,0:T(8,128)(2,1)S(1)}, u32[]{:S(2)}, u32[]{:S(2)}) collective-permute-start(bf16[4,64,2048]{2,1,0:T(8,128)(2,1)S(1)} %slice_bitcast_fusion), channel_id=1, source_target_pairs={{0,2},{2,0},{4,6},{6,4},{8,10},{10,8},{12,14},{14,12},{1,3},{3,1},... | collective-permute-start | bytes 3145736 | tf_op jit(solution)/shard_map/ppermute | solution.py:85
  167.0 26.1 %copy-start.11 = (bf16[128,2048]{1,0:T(8,128)(2,1)S(1)}, bf16[128,2048]{1,0:T(8,128)(2,1)}, u32[]{:S(2)}) copy-start(bf16[128,2048]{1,0:T(8,128)(2,1)} %param.8) | copy-start | bytes 1572868
  167.0 29.0 %copy-start.5 = (bf16[128,2048]{1,0:T(8,128)(2,1)S(1)}, bf16[128,2048]{1,0:T(8,128)(2,1)}, u32[]{:S(2)}) copy-start(bf16[128,2048]{1,0:T(8,128)(2,1)} %param.9) | copy-start | bytes 1572868
  167.1 29.0 %copy-start.18 = (f32[2048]{0:T(1024)S(1)}, f32[2048]{0:T(1024)}, u32[]{:S(2)}) copy-start(f32[2048]{0:T(1024)} %param.11) | copy-start | bytes 24580
  167.1 7.4 %collective-permute-start.25 = (bf16[64,2048]{1,0:T(8,128)(2,1)S(1)}, bf16[64,2048]{1,0:T(8,128)(2,1)S(1)}, u32[]{:S(2)}, u32[]{:S(2)}) collective-permute-start(bf16[64,2048]{1,0:T(8,128)(2,1)S(1)} %get-tuple-element.14), channel_id=1, source_target_pairs={{0,12},{2,14},{4,0},{6,2},{8,4},{10,6},{12,8},{14,10},{1,13},{3,15... | collective-permute-start | bytes 786440 | tf_op jit(solution)/shard_map/ppermute | solution.py:95
  169.5 12.7 %collective-permute-start.27 = (bf16[64,2048]{1,0:T(8,128)(2,1)S(1)}, bf16[64,2048]{1,0:T(8,128)(2,1)S(1)}, u32[]{:S(2)}, u32[]{:S(2)}) collective-permute-start(bf16[64,2048]{1,0:T(8,128)(2,1)S(1)} %get-tuple-element.15), channel_id=1, source_target_pairs={{0,4},{2,6},{4,8},{6,10},{8,12},{10,14},{12,0},{14,2},{1,5},{3,7},... | collective-permute-start | bytes 786440 | tf_op jit(solution)/shard_map/ppermute | solution.py:95
  169.5 21.3 %collective-permute-start.26 = (bf16[64,2048]{1,0:T(8,128)(2,1)S(1)}, bf16[64,2048]{1,0:T(8,128)(2,1)S(1)}, u32[]{:S(2)}, u32[]{:S(2)}) collective-permute-start(bf16[64,2048]{1,0:T(8,128)(2,1)S(1)} %get-tuple-element.16), channel_id=1, source_target_pairs={{0,8},{2,10},{4,12},{6,14},{8,0},{10,2},{12,4},{14,6},{1,9},{3,11}... | collective-permute-start | bytes 786440 | tf_op jit(solution)/shard_map/ppermute | solution.py:95
  191.0 3.3 collective-permute-start.28
  194.3 0.7 copy-start.17
  197.6 7.5 %collective-permute-start.2 = (bf16[64,2048]{1,0:T(8,128)(2,1)S(1)}, bf16[64,2048]{1,0:T(8,128)(2,1)S(1)}, u32[]{:S(2)}, u32[]{:S(2)}) collective-permute-start(bf16[64,2048]{1,0:T(8,128)(2,1)S(1)} %fusion.51), channel_id=1, source_target_pairs={{0,12},{2,14},{4,0},{6,2},{8,4},{10,6},{12,8},{14,10},{1,13},{3,15... | collective-permute-start | bytes 786440 | tf_op jit(solution)/shard_map/ppermute | solution.py:95
  199.1 18.3 %collective-permute-start.1 = (bf16[64,2048]{1,0:T(8,128)(2,1)S(1)}, bf16[64,2048]{1,0:T(8,128)(2,1)S(1)}, u32[]{:S(2)}, u32[]{:S(2)}) collective-permute-start(bf16[64,2048]{1,0:T(8,128)(2,1)S(1)} %fusion.51), channel_id=1, source_target_pairs={{0,8},{2,10},{4,12},{6,14},{8,0},{10,2},{12,4},{14,6},{1,9},{3,11}... | collective-permute-start | bytes 786440 | tf_op jit(solution)/shard_map/ppermute | solution.py:95
  200.8 22.2 %collective-permute-start = (bf16[64,2048]{1,0:T(8,128)(2,1)S(1)}, bf16[64,2048]{1,0:T(8,128)(2,1)S(1)}, u32[]{:S(2)}, u32[]{:S(2)}) collective-permute-start(bf16[64,2048]{1,0:T(8,128)(2,1)S(1)} %fusion.51), channel_id=1, source_target_pairs={{0,4},{2,6},{4,8},{6,10},{8,12},{10,14},{12,0},{14,2},{1,5},{3,7},... | collective-permute-start | bytes 786440 | tf_op jit(solution)/shard_map/ppermute | solution.py:95
  223.2 23.6 %collective-permute-start.3 = (bf16[4,64,2048]{2,1,0:T(8,128)(2,1)S(1)}, bf16[4,64,2048]{2,1,0:T(8,128)(2,1)S(1)}, u32[]{:S(2)}, u32[]{:S(2)}) collective-permute-start(bf16[4,64,2048]{2,1,0:T(8,128)(2,1)S(1)} %get-tuple-element.25), channel_id=1, source_target_pairs={{0,2},{2,0},{4,6},{6,4},{8,10},{10,8},{12,14},{14,12},{1,3},{3,1},... | collective-permute-start | bytes 3145736 | tf_op jit(solution)/shard_map/ppermute | solution.py:85
  247.0 5.9 %collective-permute-start.4 = (bf16[2,4,64,2048]{3,2,1,0:T(8,128)(2,1)S(1)}, bf16[2,4,64,2048]{3,2,1,0:T(8,128)(2,1)S(1)}, u32[]{:S(2)}, u32[]{:S(2)}) collective-permute-start(bf16[2,4,64,2048]{3,2,1,0:T(8,128)(2,1)S(1)} %get-tuple-element.13), channel_id=1, source_target_pairs={{0,1},{1,0},{2,3},{3,2},{4,5},{5,4},{6,7},{7,6},{8,9},{9,8},{10,11... | collective-permute-start | bytes 6291464 | tf_op jit(solution)/shard_map/ppermute | solution.py:85
  253.0 2.4 copy-start.10
  253.0 2.4 copy-start.15
  264.1 3.4 copy-start.7
  267.0 2.3 copy-start.3
  267.0 5.2 %collective-permute-start.7 = (bf16[2,4,64,2048]{3,2,1,0:T(8,128)(2,1)S(1)}, bf16[2,4,64,2048]{3,2,1,0:T(8,128)(2,1)S(1)}, u32[]{:S(2)}, u32[]{:S(2)}) collective-permute-start(bf16[2,4,64,2048]{3,2,1,0:T(8,128)(2,1)S(1)} %bitcast.144), channel_id=1, source_target_pairs={{0,1},{1,0},{2,3},{3,2},{4,5},{5,4},{6,7},{7,6},{8,9},{9,8},{10,11... | collective-permute-start | bytes 6291464 | tf_op jit(solution)/shard_map/ppermute | solution.py:85
  269.0 1.7 copy-start.12
  270.7 13.3 %collective-permute-start.31 = (bf16[128,2048]{1,0:T(8,128)(2,1)S(1)}, bf16[128,2048]{1,0:T(8,128)(2,1)S(1)}, u32[]{:S(2)}, u32[]{:S(2)}) collective-permute-start(bf16[128,2048]{1,0:T(8,128)(2,1)S(1)} %slice.134), channel_id=1, source_target_pairs={{0,16},{16,0},{1,17},{17,1},{2,18},{18,2},{3,19},{19,3},{4,20},{20... | collective-permute-start | bytes 1572872 | tf_op jit(solution)/shard_map/ppermute | solution.py:85
  271.1 24.2 %collective-permute-start.29 = (bf16[2048,128]{1,0:T(8,128)(2,1)S(1)}, bf16[2048,128]{1,0:T(8,128)(2,1)}, u32[]{:S(2)}, u32[]{:S(2)}) collective-permute-start(bf16[2048,128]{1,0:T(8,128)(2,1)S(1)} %slice.135), channel_id=1, source_target_pairs={{0,16},{16,0},{1,17},{17,1},{2,18},{18,2},{3,19},{19,3},{4,20},{20... | collective-permute-start | bytes 1572872 | tf_op jit(solution)/shard_map/ppermute | solution.py:85
  274.1 35.8 %collective-permute-start.8 = (bf16[4,64,2048]{2,1,0:T(8,128)(2,1)}, bf16[4,64,2048]{2,1,0:T(8,128)(2,1)}, u32[]{:S(2)}, u32[]{:S(2)}) collective-permute-start(bf16[4,64,2048]{2,1,0:T(8,128)(2,1)} %slice_bitcast_fusion.2), channel_id=1, source_target_pairs={{0,2},{2,0},{4,6},{6,4},{8,10},{10,8},{12,14},{14,12},{1,3},{3,1},... | collective-permute-start | bytes 3145736 | tf_op jit(solution)/shard_map/ppermute | solution.py:85
  285.0 18.2 %all-to-all-start.3 = ((bf16[8,128,256]{2,1,0:T(8,128)(2,1)}), bf16[8,128,256]{2,1,0:T(8,128)(2,1)}, u32[]{:S(2)}, u32[]{:S(2)}) async-start(bf16[8,128,256]{2,1,0:T(8,128)(2,1)} %bitcast.125), calls=%async_computation.3 | async-start | bytes 1048576 | tf_op jit(solution)/shard_map/all_to_all | solution.py:177
  303.1 21.7 %all-to-all-start.2 = ((bf16[8,256,128]{2,1,0:T(8,128)(2,1)}), bf16[8,256,128]{2,1,0:T(8,128)(2,1)}, u32[]{:S(2)}, u32[]{:S(2)}) async-start(bf16[8,256,128]{2,1,0:T(8,128)(2,1)} %bitcast.62), calls=%async_computation.2 | async-start | bytes 1048576 | tf_op jit(solution)/shard_map/all_to_all | solution.py:175
  309.6 15.5 %collective-permute-start.32 = (bf16[8,128,256]{2,1,0:T(8,128)(2,1)}, bf16[8,128,256]{2,1,0:T(8,128)(2,1)}, u32[]{:S(2)}, u32[]{:S(2)}) collective-permute-start(bf16[8,128,256]{2,1,0:T(8,128)(2,1)} %all-to-all-done.3), channel_id=1, source_target_pairs={{0,16},{16,0},{1,17},{17,1},{2,18},{18,2},{3,19},{19,3},{4,20},{20... | collective-permute-start | bytes 1572872 | tf_op jit(solution)/shard_map/ppermute | solution.py:85
  311.6 27.0 %collective-permute-start.9 = (bf16[64,2048]{1,0:T(8,128)(2,1)S(1)}, bf16[64,2048]{1,0:T(8,128)(2,1)S(1)}, u32[]{:S(2)}, u32[]{:S(2)}) collective-permute-start(bf16[64,2048]{1,0:T(8,128)(2,1)S(1)} %get-tuple-element.21), channel_id=1, source_target_pairs={{0,12},{2,14},{4,0},{6,2},{8,4},{10,6},{12,8},{14,10},{1,13},{3,15... | collective-permute-start | bytes 786440 | tf_op jit(solution)/shard_map/ppermute | solution.py:95
  311.6 27.0 %collective-permute-start.11 = (bf16[64,2048]{1,0:T(8,128)(2,1)S(1)}, bf16[64,2048]{1,0:T(8,128)(2,1)S(1)}, u32[]{:S(2)}, u32[]{:S(2)}) collective-permute-start(bf16[64,2048]{1,0:T(8,128)(2,1)S(1)} %get-tuple-element.22), channel_id=1, source_target_pairs={{0,4},{2,6},{4,8},{6,10},{8,12},{10,14},{12,0},{14,2},{1,5},{3,7},... | collective-permute-start | bytes 786440 | tf_op jit(solution)/shard_map/ppermute | solution.py:95
  313.1 29.6 %collective-permute-start.10 = (bf16[64,2048]{1,0:T(8,128)(2,1)S(1)}, bf16[64,2048]{1,0:T(8,128)(2,1)S(1)}, u32[]{:S(2)}, u32[]{:S(2)}) collective-permute-start(bf16[64,2048]{1,0:T(8,128)(2,1)S(1)} %get-tuple-element.23), channel_id=1, source_target_pairs={{0,8},{2,10},{4,12},{6,14},{8,0},{10,2},{12,4},{14,6},{1,9},{3,11}... | collective-permute-start | bytes 786440 | tf_op jit(solution)/shard_map/ppermute | solution.py:95
  324.8 21.1 %collective-permute-start.30 = (bf16[8,256,128]{2,1,0:T(8,128)(2,1)}, bf16[8,256,128]{2,1,0:T(8,128)(2,1)S(1)}, u32[]{:S(2)}, u32[]{:S(2)}) collective-permute-start(bf16[8,256,128]{2,1,0:T(8,128)(2,1)} %all-to-all-done.2), channel_id=1, source_target_pairs={{0,16},{16,0},{1,17},{17,1},{2,18},{18,2},{3,19},{19,3},{4,20},{20... | collective-permute-start | bytes 1572872 | tf_op jit(solution)/shard_map/ppermute | solution.py:85
  325.1 19.3 %copy-start.8 = (f32[2048,256]{1,0:T(8,128)S(1)}, f32[2048,256]{1,0:T(8,128)}, u32[]{:S(2)}) copy-start(f32[2048,256]{1,0:T(8,128)} %param.15) | copy-start | bytes 6291460
  342.8 13.7 %collective-permute-start.12 = (bf16[64,2048]{1,0:T(8,128)(2,1)S(1)}, bf16[64,2048]{1,0:T(8,128)(2,1)}, u32[]{:S(2)}, u32[]{:S(2)}) collective-permute-start(bf16[64,2048]{1,0:T(8,128)(2,1)S(1)} %fusion.28), channel_id=1, source_target_pairs={{0,1},{1,0},{2,3},{3,2},{4,5},{5,4},{6,7},{7,6},{8,9},{9,8},{10,11... | collective-permute-start | bytes 786440 | tf_op jit(solution)/shard_map/ppermute | solution.py:85
  353.3 5.2 %copy-start.1 = (bf16[2048,256]{1,0:T(8,128)(2,1)S(1)}, bf16[2048,256]{1,0:T(8,128)(2,1)}, u32[]{:S(2)}) copy-start(bf16[2048,256]{1,0:T(8,128)(2,1)} %param.13) | copy-start | bytes 3145732

commit v2 on v1

--- a/solution.py
+++ b/solution.py
@@ -1,9 +1,14 @@
+import functools
+
 import jax
 import jax.numpy as jnp
 from jax import lax
+from jax.experimental import pallas as pl
+from jax.experimental.pallas import tpu as pltpu
 from jax.sharding import PartitionSpec as P
 
 EPSILON = 1e-06
+MESH = pl.DeviceIdType.MESH
 TRANSPOSED = (((1,), (1,)), ((), ()))
 LEADING = (((0,), (0,)), ((), ()))
 
@@ -101,15 +106,6 @@
     return jnp.where(axis_index == 0, jnp.stack([first, second]), jnp.stack([second, first]))
 
 
-def gather_tokens(values):
-    rows, width = values.shape
-    outer = lax.axis_size("fs") // 2
-    half = own_half(values.reshape(2, rows // 2, width), lax.axis_index("tp"), 0)
-    line = jnp.stack([half] + [line_shift(half, s) for s in range(1, outer)])
-    both = jnp.stack([line, swap(line, "fs")])
-    return jnp.stack([both, swap(both, "tp")]).reshape(-1, width)
-
-
 def scatter_tokens(partial, rows):
     width = partial.shape[1]
     outer = lax.axis_size("fs") // 2
@@ -118,12 +114,214 @@
     blocks = (blocks[0].astype(jnp.float32) + got.astype(jnp.float32)).astype(jnp.bfloat16)
     got = swap(blocks[1], "fs")
     blocks = (blocks[0].astype(jnp.float32) + got.astype(jnp.float32)).astype(jnp.bfloat16)
-    total = blocks[0].astype(jnp.float32)
+    place = lax.axis_index("fs") // 2
+    total = own_half(blocks, place, 0).astype(jnp.float32)
     for s in range(1, outer):
-        total = total + line_shift(blocks[s], -s).astype(jnp.float32)
+        sent = own_half(blocks, (place + s) % outer, 0)
+        total = total + line_shift(sent, s).astype(jnp.float32)
     half = total.astype(jnp.bfloat16)
     whole = ordered(half, swap(half, "tp"), lax.axis_index("tp"))
     return whole.reshape(rows, width).astype(jnp.float32)
+
+
+def gather_kernel(
+    n_fs, own, up, down, tok, up_out, down_out,
+    line_send, line_recv, pair_send, pair_recv, core_send, core_recv,
+    weight_send, weight_recv, local_sem,
+):
+    rep, fs, core = lax.axis_index("rep"), lax.axis_index("fs"), lax.axis_index("tp")
+    outer = n_fs // 2
+    place = fs // 2
+    pair = fs % 2
+    depth, units = up.shape
+    own_units = units // n_fs
+    part = own_units // 2
+    other_pair = (rep, place * 2 + 1 - pair, core)
+    other_core = (rep, fs, 1 - core)
+    other_rep = (1 - rep, fs, core)
+
+    barrier = pltpu.get_barrier_semaphore()
+    peers = [other_core, other_rep]
+    peers += [(rep, lax.rem(fs + k, n_fs), core) for k in range(1, n_fs)]
+    for peer in peers:
+        pl.semaphore_signal(barrier, inc=1, device_id=peer, device_id_type=MESH)
+    pl.semaphore_wait(barrier, len(peers))
+
+    def copy(source, target, send, recv, device):
+        return pltpu.make_async_remote_copy(
+            src_ref=source, dst_ref=target, send_sem=send, recv_sem=recv,
+            device_id=device, device_id_type=MESH,
+        )
+
+    def slot(other, far, index):
+        return tok.at[:, other, far, index]
+
+    def to_line(source, index, way):
+        step = 1 if way else -1
+        target = (rep, fs + 2 * step, core)
+        return copy(source, slot(0, 0, index), line_send.at[way, index], line_recv.at[index], target)
+
+    def to_pair(source, index):
+        return copy(
+            source, slot(0, 1, index), pair_send.at[index], pair_recv.at[index], other_pair
+        )
+
+    def to_core(source, far, index):
+        return copy(
+            source, slot(1, far, index), core_send.at[far, index], core_recv.at[far, index],
+            other_core,
+        )
+
+    def up_source(k):
+        start = pl.multiple_of(k * own_units + rep * part, part)
+        return up.at[:, pl.ds(start, part)]
+
+    def down_source(k):
+        start = pl.multiple_of(k * own_units + rep * part, part)
+        return down.at[pl.ds(start, part), :]
+
+    def up_slot(k, half):
+        return up_out.at[k, :, half * part : (half + 1) * part]
+
+    def down_slot(k, half):
+        columns = pl.ds(pl.multiple_of(k * depth, depth), depth)
+        return down_out.at[half * part : (half + 1) * part, columns]
+
+    def up_copy(k):
+        return copy(
+            up_source(k), up_slot(fs, 0), weight_send.at[0, 0, k], weight_recv.at[0, 0, fs],
+            (rep, k, core),
+        )
+
+    def down_copy(k):
+        return copy(
+            down_source(k), down_slot(fs, 0), weight_send.at[0, 1, k], weight_recv.at[0, 1, fs],
+            (rep, k, core),
+        )
+
+    def up_pass(source, k):
+        return copy(
+            source, up_slot(k, 1), weight_send.at[1, 0, k], weight_recv.at[1, 0, k], other_rep
+        )
+
+    def down_pass(source, k):
+        return copy(
+            source, down_slot(k, 1), weight_send.at[1, 1, k], weight_recv.at[1, 1, k], other_rep
+        )
+
+    def landed(target, sem):
+        copy(target, target, sem, sem, other_core).wait_recv()
+
+    @pl.when(place > 0)
+    def _():
+        to_line(own, place, 0).start()
+
+    @pl.when(place < outer - 1)
+    def _():
+        to_line(own, place, 1).start()
+
+    to_pair(own, place).start()
+    to_core(own, 0, place).start()
+    keep = [
+        pltpu.make_async_copy(own, slot(0, 0, place), local_sem.at[0]),
+        pltpu.make_async_copy(up_source(fs), up_slot(fs, 0), local_sem.at[1]),
+        pltpu.make_async_copy(down_source(fs), down_slot(fs, 0), local_sem.at[2]),
+    ]
+    for one in keep:
+        one.start()
+    up_pass(up_source(fs), fs).start()
+    down_pass(down_source(fs), fs).start()
+    for k in range(1, n_fs):
+        peer = lax.rem(fs + k, n_fs)
+        up_copy(peer).start()
+        down_copy(peer).start()
+
+    for d in range(1, outer):
+        if d == outer - 1:
+            for k in range(1, n_fs):
+                peer = lax.rem(fs + n_fs - k, n_fs)
+                landed(up_slot(peer, 0), weight_recv.at[0, 0, peer])
+                up_pass(up_slot(peer, 0), peer).start()
+                landed(down_slot(peer, 0), weight_recv.at[0, 1, peer])
+                down_pass(down_slot(peer, 0), peer).start()
+        for way in range(2):
+            index = place - d if way else place + d
+            there = index >= 0 if way else index < outer
+            more = place < outer - 1 if way else place > 0
+
+            @pl.when(there)
+            def _(index=index, way=way, more=more):
+                landed(slot(0, 0, index), line_recv.at[index])
+
+                @pl.when(more)
+                def _():
+                    to_line(slot(0, 0, index), index, way).start()
+
+                to_pair(slot(0, 0, index), index).start()
+                to_core(slot(0, 0, index), 0, index).start()
+
+    def pass_pair(index):
+        landed(slot(0, 1, index), pair_recv.at[index])
+        to_core(slot(0, 1, index), 1, index).start()
+
+    pass_pair(place)
+    for d in range(1, outer):
+        for way in range(2):
+            index = place - d if way else place + d
+
+            @pl.when(index >= 0 if way else index < outer)
+            def _(index=index):
+                pass_pair(index)
+
+    for one in keep:
+        one.wait()
+    for k in range(n_fs):
+        landed(up_slot(k, 1), weight_recv.at[1, 0, k])
+        landed(down_slot(k, 1), weight_recv.at[1, 1, k])
+        up_pass(up_slot(k, 0), k).wait_send()
+        down_pass(down_slot(k, 0), k).wait_send()
+    for k in range(1, n_fs):
+        peer = lax.rem(fs + k, n_fs)
+        up_copy(peer).wait_send()
+        down_copy(peer).wait_send()
+    for index in range(outer):
+        to_pair(own, index).wait_send()
+        for far in range(2):
+            landed(slot(1, far, index), core_recv.at[far, index])
+            to_core(own, far, index).wait_send()
+
+        @pl.when(jnp.logical_and(index >= place, place > 0))
+        def _(index=index):
+            to_line(own, index, 0).wait_send()
+
+        @pl.when(jnp.logical_and(index <= place, place < outer - 1))
+        def _(index=index):
+            to_line(own, index, 1).wait_send()
+
+
+def gather_all(blocks, up_weight, down_weight):
+    n_fs = lax.axis_size("fs")
+    outer = n_fs // 2
+    arrays, rows, width = blocks.shape
+    depth, units = up_weight.shape
+    own_units = units // n_fs
+    dma = pltpu.SemaphoreType.DMA
+    tok, up_own, down_own = pl.pallas_call(
+        functools.partial(gather_kernel, n_fs),
+        out_shape=(
+            jax.ShapeDtypeStruct((arrays, 2, 2, outer, rows, width), blocks.dtype),
+            jax.ShapeDtypeStruct((n_fs, depth, own_units), up_weight.dtype),
+            jax.ShapeDtypeStruct((own_units, n_fs * depth), down_weight.dtype),
+        ),
+        in_specs=[pl.BlockSpec(memory_space=pl.ANY)] * 3,
+        out_specs=[pl.BlockSpec(memory_space=pl.ANY)] * 3,
+        scratch_shapes=[
+            dma((2, outer)), dma((outer,)), dma((outer,)), dma((outer,)),
+            dma((2, outer)), dma((2, outer)), dma((2, 2, n_fs)), dma((2, 2, n_fs)), dma((3,)),
+        ],
+        compiler_params=pltpu.CompilerParams(collective_id=0, has_side_effects=True),
+    )(blocks, up_weight, down_weight)
+    return tok, up_own.reshape(n_fs * depth, own_units), down_own
 
 
 def hidden_body(
@@ -140,18 +338,16 @@
         kept_input_rows, norm_gain_vector
     )
     part = own_units // 2
-    up_half = own_half(up_weight.reshape(depth, n_fs, 2, part), group, 2)
-    down_half = own_half(down_weight.reshape(n_fs, 2, part, depth), group, 1)
-    up_half = lax.all_to_all(up_half.transpose(1, 0, 2), "fs", 0, 0, tiled=True)
-    down_half = lax.all_to_all(down_half, "fs", 0, 0, tiled=True)
-    up_half = up_half.reshape(width, part)
-    down_half = down_half.transpose(1, 0, 2).reshape(part, width)
-    up_own = jnp.concatenate([up_half, swap(up_half, "rep")], axis=1)
-    down_own = jnp.concatenate([down_half, swap(down_half, "rep")], axis=0)
-
-    normed_saved = gather_tokens(normed_kept_rows)
-    cot = gather_tokens(cotangent)
-    normed_next = gather_tokens(normed_later)
+    part = own_units // 2
+    core = lax.axis_index("tp")
+    blocks = jnp.stack(
+        [
+            own_half(values.reshape(2, row_count // 2, width), core, 0)
+            for values in (normed_kept_rows, cotangent, normed_later)
+        ]
+    )
+    tok, up_own, down_own = gather_all(blocks, up_weight, down_weight)
+    normed_saved, cot, normed_next = (tok[i].reshape(-1, width) for i in range(3))
 
     pre_saved = jnp.dot(normed_saved, up_own, preferred_element_type=jnp.float32)
     hidden_saved = squared_relu(pre_saved)

time: 363 us -> 255 us (0.70); the launches traced: 358 us -> 255 us
  waiting for transfers between devices: 200 us -> 56.2 us
  Pallas kernels: 0 us -> 87.3 us
  starting transfers between devices: 79.7 us -> 43.4 us
  other arithmetic: 39.5 us -> 25.4 us
    pallas_call x0 -> x1, Pallas kernels: none -> 87.3 us  [gather_all(): pl.pallas_call(functools.partial(gather_kernel, n_fs), out_shape=(jax.Sha...]
    ppermute x15 -> x6, waiting for transfers between devices: 87.2 us -> 19.2 us  [line_shift(): lax.ppermute(values, 'fs', [(i, (i // 2 + shift) % outer * 2 + i % 2) for...]
    ppermute x18 -> x10, waiting for transfers between devices: 87.5 us -> 33.2 us  [swap(): return lax.ppermute(values, axis, [(i, i ^ 1) for i in range(size)])]
    ppermute x18 -> x10, starting transfers between devices: 30.2 us -> 10.8 us  [swap(): return lax.ppermute(values, axis, [(i, i ^ 1) for i in range(size)])]
    another operation x9 -> x1, other arithmetic: 18 us -> 0.97 us  [hidden_body(): jnp.stack([own_half(values.reshape(2, row_count // 2, width), core, 0) fo...]
    ppermute x15 -> x6, starting transfers between devices: 25.3 us -> 9 us  [line_shift(): lax.ppermute(values, 'fs', [(i, (i // 2 + shift) % outer * 2 + i % 2) for...]
    all_to_all x1 -> x0, waiting for transfers between devices: 11.5 us -> none  [hidden_body(): up_half = lax.all_to_all(up_half.transpose(1, 0, 2), 'fs', 0, 0, tiled=True)]
    slice x0 -> x1, local copies, waits for them, and re-layouts: none -> 7.2 us  [hidden_body(): tok[i].reshape(-1, width)]
  transfers between devices with their start and end apart: 37 -> 18, of which waited for: 26 -> 7; matrix products, arithmetic and copies ran while one was open for 14% -> 20% of each run, Pallas kernels for 0% -> 0%
where the time goes in v2:
time: 255 us
  Pallas kernels  87.3 us (34%)
  waiting for transfers between devices  56.2 us (22%)
  starting transfers between devices  43.4 us (17%)
  local copies, waits for them, and re-layouts  25.8 us (10%)
  other arithmetic  25.4 us (10%)
  matrix products  15.6 us (6%)
    pallas_call x1, Pallas kernels, gather_all(): pl.pallas_call(functools.partial(gather_kernel, n_fs), out_shape=(jax.Sha...  87.3 us
    ppermute x10, waiting for transfers between devices, swap(): return lax.ppermute(values, axis, [(i, i ^ 1) for i in range(size)])  33.2 us
    ppermute x6, waiting for transfers between devices, line_shift(): lax.ppermute(values, 'fs', [(i, (i // 2 + shift) % outer * 2 + i % 2) for...  19.2 us
    all_to_all x1, starting transfers between devices, hidden_body(): down_half = lax.all_to_all(down_half, 'fs', 0, 0, tiled=True)  17.5 us
    ppermute x10, starting transfers between devices, swap(): return lax.ppermute(values, axis, [(i, i ^ 1) for i in range(size)])  10.8 us
    dot_general x1, matrix products, hidden_body(): jnp.dot(hidden_later, down_own, preferred_element_type=jnp.float32)  9.08 us
    ppermute x6, starting transfers between devices, line_shift(): lax.ppermute(values, 'fs', [(i, (i // 2 + shift) % outer * 2 + i % 2) for...  9 us
    convert_element_type x4, other arithmetic, scatter_tokens(): (blocks[0].astype(jnp.float32) + got.astype(jnp.float32)).astype(jnp.bflo...  7.97 us
  transfers between devices with their start and end apart: 18, of which 7 were waited for; matrix products, arithmetic and copies ran while one was open for 20% of the time, Pallas kernels for 0%

profile of v2, /device:TPU:11, one launch (start us, length us, event | category | flops | bytes accessed | tf_op | source)
XLA Modules:
  0.0 254.8 jit_solution(15297363154464158835)
XLA Ops:
  0.7 1.3 fusion.16
  1.9 1.2 fusion.17
  3.2 1.5 fusion.11
  4.8 1.0 pad_maximum_fusion.own
  5.8 87.3 %shard_map.111 = (bf16[3,2,2,4,64,2048]{5,4,3,2,1,0:T(8,128)(2,1)}, bf16[8,256,256]{2,1,0:T(8,128)(2,1)}, bf16[256,2048]{1,0:T(8,128)(2,1)}) custom-call(bf16[3,64,2048]{2,1,0:T(8,128)(2,1)} %pad_maximum_fusion.own, bf16[256,2048]{1,0:T(8,128)(2,1)} %up.1, bf16[2048,256]{1,0:T(8,128)(2,1)} %down.1), custom_call_target="tpu_custom_call" | custom-call | tf_op jit(solution)/shard_map/pallas_call | solution.py:309
  93.1 7.2 %fusion.31 = (bf16[1,2,2,4,64,2048]{5,4,3,2,1,0:T(8,128)(2,1)S(1)}, bf16[1,2,2,4,64,2048]{5,4,3,2,1,0:T(8,128)(2,1)S(1)}, bf16[1,2,2,4,64,2048]{5,4,3,2,1,0:T(8,128)(2,1)}) fusion(bf16[3,2,2,4,64,2048]{5,4,3,2,1,0:T(8,128)(2,1)} %get-tuple-element.7), kind=kLoop, calls=%fused_computation.78 | loop fusion | bytes 25165824 | tf_op jit(solution)/shard_map/slice | solution.py:350
  100.3 1.3 convolution_maximum_fusion
  101.5 1.3 convolution_multiply_fusion
  102.9 0.3 collective-permute-start.14
  103.2 1.4 fusion.9
  104.6 1.4 convolution_multiply_fusion.1
  106.0 0.9 slice.95
  106.9 0.6 copy-done.7
  107.5 1.2 collective-permute-start.12
  108.7 1.3 convolution_convert_fusion
  110.0 1.8 fusion.32
  111.8 0.7 collective-permute-start.6
  112.5 3.9 %collective-permute-done.14 = bf16[128,2048]{1,0:T(8,128)(2,1)S(1)} collective-permute-done((bf16[128,2048]{1,0:T(8,128)(2,1)S(1)}, bf16[128,2048]{1,0:T(8,128)(2,1)S(1)}, u32[]{:S(2)}, u32[]{:S(2)}) %collective-permute-start.14) | collective-permute-done | bytes 524320 | tf_op jit(solution)/shard_map/ppermute | solution.py:90
  116.3 0.1 fusion.20
  116.5 0.8 copy.20
  117.3 17.5 %all-to-all-start.1 = ((bf16[8,128,256]{2,1,0:T(8,128)(2,1)}), bf16[8,128,256]{2,1,0:T(8,128)(2,1)S(1)}, u32[]{:S(2)}, u32[]{:S(2)}) async-start(bf16[8,128,256]{2,1,0:T(8,128)(2,1)} %bitcast.83), calls=%async_computation.1 | async-start | bytes 1048576 | tf_op jit(solution)/shard_map/all_to_all | solution.py:373
  134.8 9.1 %convolution_convert_fusion.1 = bf16[1024,2048]{1,0:T(8,128)(2,1)} fusion(bf16[256,2048]{1,0:T(8,128)(2,1)} %get-tuple-element.9, bf16[1024,2048]{1,0:T(8,128)(2,1)} %bitcast.89, bf16[2048,256]{1,0:T(8,128)(2,1)} %bitcast.98), kind=kOutput, calls=%fused_computation.5 | convolution fusion | flops 2150367232 | bytes 10485760 | tf_op jit(solution)/shard_map/dot_general | solution.py:368
  143.9 2.3 fusion.21
  146.2 6.1 %all-to-all-start = ((bf16[8,256,128]{2,1,0:T(8,128)(2,1)}), bf16[8,256,128]{2,1,0:T(8,128)(2,1)S(1)}, u32[]{:S(2)}, u32[]{:S(2)}) async-start(bf16[8,256,128]{2,1,0:T(8,128)(2,1)} %bitcast.94), calls=%async_computation | async-start | bytes 1048576 | tf_op jit(solution)/shard_map/all_to_all | solution.py:371
  152.2 4.8 %fusion.33 = (bf16[512,2048]{1,0:T(8,128)(2,1)}, bf16[512,2048]{1,0:T(8,128)(2,1)}) fusion(bf16[1024,2048]{1,0:T(8,128)(2,1)} %convolution_convert_fusion.1), kind=kLoop, calls=%fused_computation.80 | loop fusion | bytes 8388608 | tf_op jit(solution)/shard_map/slice | solution.py:113
  157.1 2.1 collective-permute-start
  159.1 0.3 collective-permute-start.15
  159.4 3.8 %all-to-all-done = bf16[8,256,128]{2,1,0:T(8,128)(2,1)S(1)} async-done(((bf16[8,256,128]{2,1,0:T(8,128)(2,1)}), bf16[8,256,128]{2,1,0:T(8,128)(2,1)S(1)}, u32[]{:S(2)}, u32[]{:S(2)}) %all-to-all-start) | async-done | bytes 524320 | tf_op jit(solution)/shard_map/all_to_all | solution.py:371
  163.2 0.3 collective-permute-start.13
  163.4 9.3 %collective-permute-done.15 = bf16[8,128,256]{2,1,0:T(8,128)(2,1)} collective-permute-done((bf16[8,128,256]{2,1,0:T(8,128)(2,1)S(1)}, bf16[8,128,256]{2,1,0:T(8,128)(2,1)}, u32[]{:S(2)}, u32[]{:S(2)}) %collective-permute-start.15) | collective-permute-done | bytes 524320 | tf_op jit(solution)/shard_map/ppermute | solution.py:90
  172.7 1.4 fusion.22
  174.1 2.4 fusion
  176.5 1.1 slice_bitcast_fusion
  177.6 1.2 collective-permute-start.7
  178.8 0.4 copy-done.4
  179.2 2.4 fusion.1
  181.6 1.0 slice_bitcast_fusion.2
  182.6 1.2 collective-permute-start.1
  183.8 1.8 bitcast_add_fusion
  185.6 0.2 convert_bitcast_fusion
  185.8 2.9 %copy.16 = f32[256,8,2,128]{3,2,1,0:T(2,128)} copy(f32[256,8,2,128]{3,0,1,2:T(8,128)S(1)} %convert_bitcast_fusion) | data formatting | bytes 4194304 | tf_op jit(solution)/shard_map/convert_element_type | solution.py:392
  188.7 3.9 %reshape.100 = f32[256,2048]{1,0:T(8,128)} reshape(f32[256,8,2,128]{3,2,1,0:T(2,128)} %copy.16) | data formatting | bytes 4194304 | tf_op jit(solution)/shard_map/convert_element_type | solution.py:392
  192.6 4.0 %add.131 = f32[256,2048]{1,0:T(8,128)} add(f32[256,2048]{1,0:T(8,128)} %param.14, f32[256,2048]{1,0:T(8,128)} %reshape.100) | non-fusion elementwise | flops 524288 | bytes 6291456 | tf_op jit(solution)/shard_map/add | solution.py:392
  196.6 4.7 %collective-permute-done.7 = bf16[4,64,2048]{2,1,0:T(8,128)(2,1)} collective-permute-done((bf16[4,64,2048]{2,1,0:T(8,128)(2,1)}, bf16[4,64,2048]{2,1,0:T(8,128)(2,1)}, u32[]{:S(2)}, u32[]{:S(2)}) %collective-permute-start.7) | collective-permute-done | bytes 1048608 | tf_op jit(solution)/shard_map/ppermute | solution.py:90
  201.3 1.6 fusion.2
  203.0 0.1 dynamic-slice_bitcast_fusion.2
  203.1 0.3 collective-permute-start.10
  203.4 1.2 collective-permute-start.8
  204.6 3.9 %collective-permute-start.9 = (bf16[64,2048]{1,0:T(8,128)(2,1)S(1)}, bf16[64,2048]{1,0:T(8,128)(2,1)S(1)}, u32[]{:S(2)}, u32[]{:S(2)}) collective-permute-start(bf16[64,2048]{1,0:T(8,128)(2,1)S(1)} %get-tuple-element.19), channel_id=1, source_target_pairs={{0,8},{2,10},{4,12},{6,14},{8,0},{10,2},{12,4},{14,6},{1,9},{3,11}... | collective-permute-start | bytes 786440 | tf_op jit(solution)/shard_map/ppermute | solution.py:100
  208.5 15.3 %collective-permute-done.1 = bf16[4,64,2048]{2,1,0:T(8,128)(2,1)} collective-permute-done((bf16[4,64,2048]{2,1,0:T(8,128)(2,1)}, bf16[4,64,2048]{2,1,0:T(8,128)(2,1)}, u32[]{:S(2)}, u32[]{:S(2)}) %collective-permute-start.1) | collective-permute-done | bytes 1048608 | tf_op jit(solution)/shard_map/ppermute | solution.py:90
  223.8 1.6 fusion.3
  225.5 1.2 collective-permute-start.2
  226.8 1.2 collective-permute-start.3
  227.9 1.2 collective-permute-start.4
  229.1 0.1 fusion.25
  229.3 3.1 %collective-permute-start.11 = (bf16[64,2048]{1,0:T(8,128)(2,1)S(1)}, bf16[64,2048]{1,0:T(8,128)(2,1)S(1)}, u32[]{:S(2)}, u32[]{:S(2)}) collective-permute-start(bf16[64,2048]{1,0:T(8,128)(2,1)S(1)} %fusion.25), channel_id=1, source_target_pairs={{0,1},{1,0},{2,3},{3,2},{4,5},{5,4},{6,7},{7,6},{8,9},{9,8},{10,11... | collective-permute-start | bytes 786440 | tf_op jit(solution)/shard_map/ppermute | solution.py:90
  232.4 15.3 %collective-permute-done.3 = bf16[64,2048]{1,0:T(8,128)(2,1)S(1)} collective-permute-done((bf16[64,2048]{1,0:T(8,128)(2,1)S(1)}, bf16[64,2048]{1,0:T(8,128)(2,1)S(1)}, u32[]{:S(2)}, u32[]{:S(2)}) %collective-permute-start.3) | collective-permute-done | bytes 262176 | tf_op jit(solution)/shard_map/ppermute | solution.py:100
  247.7 3.9 %collective-permute-done.4 = bf16[64,2048]{1,0:T(8,128)(2,1)S(1)} collective-permute-done((bf16[64,2048]{1,0:T(8,128)(2,1)S(1)}, bf16[64,2048]{1,0:T(8,128)(2,1)S(1)}, u32[]{:S(2)}, u32[]{:S(2)}) %collective-permute-start.4) | collective-permute-done | bytes 262176 | tf_op jit(solution)/shard_map/ppermute | solution.py:100
  251.6 0.1 fusion.28
  251.7 0.6 collective-permute-start.5
  252.3 0.1 maximum_select_fusion.3
  252.4 0.3 fusion.12
  252.8 1.2 fusion.15
  253.9 0.9 maximum_select_fusion.2
  (38 shorter events, 0.3 us)
Async XLA Ops:
  0.6 4.2 %copy-start = (bf16[128,2048]{1,0:T(8,128)(2,1)S(1)}, bf16[128,2048]{1,0:T(8,128)(2,1)}, u32[]{:S(2)}) copy-start(bf16[128,2048]{1,0:T(8,128)(2,1)} %param.10) | copy-start | bytes 1572868
  93.1 7.2 %copy-start.8 = (bf16[8,256,256]{2,1,0:T(8,128)(2,1)S(1)}, bf16[8,256,256]{2,1,0:T(8,128)(2,1)}, u32[]{:S(2)}) copy-start(bf16[8,256,256]{2,1,0:T(8,128)(2,1)} %get-tuple-element.8) | copy-start | bytes 3145732
  101.5 1.7 copy-start.10
  102.9 13.4 %collective-permute-start.14 = (bf16[128,2048]{1,0:T(8,128)(2,1)S(1)}, bf16[128,2048]{1,0:T(8,128)(2,1)S(1)}, u32[]{:S(2)}, u32[]{:S(2)}) collective-permute-start(bf16[128,2048]{1,0:T(8,128)(2,1)S(1)} %slice.94), channel_id=1, source_target_pairs={{0,16},{16,0},{1,17},{17,1},{2,18},{18,2},{3,19},{19,3},{4,20},{20... | collective-permute-start | bytes 1572872 | tf_op jit(solution)/shard_map/ppermute | solution.py:90
  106.0 1.5 copy-start.7
  107.5 36.4 %collective-permute-start.12 = (bf16[2048,128]{1,0:T(8,128)(2,1)}, bf16[2048,128]{1,0:T(8,128)(2,1)}, u32[]{:S(2)}, u32[]{:S(2)}) collective-permute-start(bf16[2048,128]{1,0:T(8,128)(2,1)} %slice.95), channel_id=1, source_target_pairs={{0,16},{16,0},{1,17},{17,1},{2,18},{18,2},{3,19},{19,3},{4,20},{20... | collective-permute-start | bytes 1572872 | tf_op jit(solution)/shard_map/ppermute | solution.py:90
  111.8 62.3 %collective-permute-start.6 = (bf16[2,4,64,2048]{3,2,1,0:T(8,128)(2,1)}, bf16[2,4,64,2048]{3,2,1,0:T(8,128)(2,1)}, u32[]{:S(2)}, u32[]{:S(2)}) collective-permute-start(bf16[2,4,64,2048]{3,2,1,0:T(8,128)(2,1)} %bitcast.19), channel_id=1, source_target_pairs={{0,1},{1,0},{2,3},{3,2},{4,5},{5,4},{6,7},{7,6},{8,9},{9,8},{10,11... | collective-permute-start | bytes 6291464 | tf_op jit(solution)/shard_map/ppermute | solution.py:90
  117.3 28.9 %all-to-all-start.1 = ((bf16[8,128,256]{2,1,0:T(8,128)(2,1)}), bf16[8,128,256]{2,1,0:T(8,128)(2,1)S(1)}, u32[]{:S(2)}, u32[]{:S(2)}) async-start(bf16[8,128,256]{2,1,0:T(8,128)(2,1)} %bitcast.83), calls=%async_computation.1 | async-start | bytes 1048576 | tf_op jit(solution)/shard_map/all_to_all | solution.py:373
  146.2 17.0 %all-to-all-start = ((bf16[8,256,128]{2,1,0:T(8,128)(2,1)}), bf16[8,256,128]{2,1,0:T(8,128)(2,1)S(1)}, u32[]{:S(2)}, u32[]{:S(2)}) async-start(bf16[8,256,128]{2,1,0:T(8,128)(2,1)} %bitcast.94), calls=%async_computation | async-start | bytes 1048576 | tf_op jit(solution)/shard_map/all_to_all | solution.py:371
  157.1 21.8 %collective-permute-start = (bf16[2,4,64,2048]{3,2,1,0:T(8,128)(2,1)}, bf16[2,4,64,2048]{3,2,1,0:T(8,128)(2,1)}, u32[]{:S(2)}, u32[]{:S(2)}) collective-permute-start(bf16[2,4,64,2048]{3,2,1,0:T(8,128)(2,1)} %bitcast.6), channel_id=1, source_target_pairs={{0,1},{1,0},{2,3},{3,2},{4,5},{5,4},{6,7},{7,6},{8,9},{9,8},{10,11... | collective-permute-start | bytes 6291464 | tf_op jit(solution)/shard_map/ppermute | solution.py:90
  159.1 13.6 %collective-permute-start.15 = (bf16[8,128,256]{2,1,0:T(8,128)(2,1)S(1)}, bf16[8,128,256]{2,1,0:T(8,128)(2,1)}, u32[]{:S(2)}, u32[]{:S(2)}) collective-permute-start(bf16[8,128,256]{2,1,0:T(8,128)(2,1)S(1)} %all-to-all-done.1), channel_id=1, source_target_pairs={{0,16},{16,0},{1,17},{17,1},{2,18},{18,2},{3,19},{19,3},{4,20},{20... | collective-permute-start | bytes 1572872 | tf_op jit(solution)/shard_map/ppermute | solution.py:90
  163.2 22.4 %collective-permute-start.13 = (bf16[8,256,128]{2,1,0:T(8,128)(2,1)S(1)}, bf16[8,256,128]{2,1,0:T(8,128)(2,1)S(1)}, u32[]{:S(2)}, u32[]{:S(2)}) collective-permute-start(bf16[8,256,128]{2,1,0:T(8,128)(2,1)S(1)} %all-to-all-done), channel_id=1, source_target_pairs={{0,16},{16,0},{1,17},{17,1},{2,18},{18,2},{3,19},{19,3},{4,20},{20... | collective-permute-start | bytes 1572872 | tf_op jit(solution)/shard_map/ppermute | solution.py:90
  176.5 5.1 %copy-start.2 = (bf16[2,4,64,2048]{3,2,1,0:T(8,128)(2,1)}, bf16[2,4,64,2048]{3,2,1,0:T(8,128)(2,1)S(1)}, u32[]{:S(2)}) copy-start(bf16[2,4,64,2048]{3,2,1,0:T(8,128)(2,1)S(1)} %fusion) | copy-start | bytes 6291460
  176.5 2.7 %copy-start.4 = (bf16[512,2048]{1,0:T(8,128)(2,1)S(1)}, bf16[512,2048]{1,0:T(8,128)(2,1)}, u32[]{:S(2)}) copy-start(bf16[512,2048]{1,0:T(8,128)(2,1)} %get-tuple-element.16) | copy-start | bytes 6291460
  177.6 23.7 %collective-permute-start.7 = (bf16[4,64,2048]{2,1,0:T(8,128)(2,1)}, bf16[4,64,2048]{2,1,0:T(8,128)(2,1)}, u32[]{:S(2)}, u32[]{:S(2)}) collective-permute-start(bf16[4,64,2048]{2,1,0:T(8,128)(2,1)} %slice_bitcast_fusion), channel_id=1, source_target_pairs={{0,2},{2,0},{4,6},{6,4},{8,10},{10,8},{12,14},{14,12},{1,3},{3,1},... | collective-permute-start | bytes 3145736 | tf_op jit(solution)/shard_map/ppermute | solution.py:90
  181.6 2.2 copy-start.6
  182.6 41.2 %collective-permute-start.1 = (bf16[4,64,2048]{2,1,0:T(8,128)(2,1)}, bf16[4,64,2048]{2,1,0:T(8,128)(2,1)}, u32[]{:S(2)}, u32[]{:S(2)}) collective-permute-start(bf16[4,64,2048]{2,1,0:T(8,128)(2,1)} %slice_bitcast_fusion.2), channel_id=1, source_target_pairs={{0,2},{2,0},{4,6},{6,4},{8,10},{10,8},{12,14},{14,12},{1,3},{3,1},... | collective-permute-start | bytes 3145736 | tf_op jit(solution)/shard_map/ppermute | solution.py:90
  192.6 8.7 %copy-start.3 = (bf16[2,4,64,2048]{3,2,1,0:T(8,128)(2,1)S(1)}, bf16[2,4,64,2048]{3,2,1,0:T(8,128)(2,1)}, u32[]{:S(2)}) copy-start(bf16[2,4,64,2048]{3,2,1,0:T(8,128)(2,1)} %copy-done.2) | copy-start | bytes 6291460
  203.1 24.9 %collective-permute-start.10 = (bf16[64,2048]{1,0:T(8,128)(2,1)S(1)}, bf16[64,2048]{1,0:T(8,128)(2,1)S(1)}, u32[]{:S(2)}, u32[]{:S(2)}) collective-permute-start(bf16[64,2048]{1,0:T(8,128)(2,1)S(1)} %get-tuple-element.18), channel_id=1, source_target_pairs={{0,12},{2,14},{4,0},{6,2},{8,4},{10,6},{12,8},{14,10},{1,13},{3,15... | collective-permute-start | bytes 786440 | tf_op jit(solution)/shard_map/ppermute | solution.py:100
  203.4 25.7 %collective-permute-start.8 = (bf16[64,2048]{1,0:T(8,128)(2,1)S(1)}, bf16[64,2048]{1,0:T(8,128)(2,1)S(1)}, u32[]{:S(2)}, u32[]{:S(2)}) collective-permute-start(bf16[64,2048]{1,0:T(8,128)(2,1)S(1)} %get-tuple-element.17), channel_id=1, source_target_pairs={{0,4},{2,6},{4,8},{6,10},{8,12},{10,14},{12,0},{14,2},{1,5},{3,7},... | collective-permute-start | bytes 786440 | tf_op jit(solution)/shard_map/ppermute | solution.py:100
  204.6 24.6 %collective-permute-start.9 = (bf16[64,2048]{1,0:T(8,128)(2,1)S(1)}, bf16[64,2048]{1,0:T(8,128)(2,1)S(1)}, u32[]{:S(2)}, u32[]{:S(2)}) collective-permute-start(bf16[64,2048]{1,0:T(8,128)(2,1)S(1)} %get-tuple-element.19), channel_id=1, source_target_pairs={{0,8},{2,10},{4,12},{6,14},{8,0},{10,2},{12,4},{14,6},{1,9},{3,11}... | collective-permute-start | bytes 786440 | tf_op jit(solution)/shard_map/ppermute | solution.py:100
  225.5 26.9 %copy-start.5 = (bf16[128,2048]{1,0:T(8,128)(2,1)S(1)}, bf16[128,2048]{1,0:T(8,128)(2,1)}, u32[]{:S(2)}) copy-start(bf16[128,2048]{1,0:T(8,128)(2,1)} %param.9) | copy-start | bytes 1572868
  225.5 26.9 %copy-start.9 = (f32[2048]{0:T(1024)S(1)}, f32[2048]{0:T(1024)}, u32[]{:S(2)}) copy-start(f32[2048]{0:T(1024)} %param.11) | copy-start | bytes 24580
  225.5 6.8 %collective-permute-start.2 = (bf16[64,2048]{1,0:T(8,128)(2,1)S(1)}, bf16[64,2048]{1,0:T(8,128)(2,1)S(1)}, u32[]{:S(2)}, u32[]{:S(2)}) collective-permute-start(bf16[64,2048]{1,0:T(8,128)(2,1)S(1)} %get-tuple-element.20), channel_id=1, source_target_pairs={{0,4},{2,6},{4,8},{6,10},{8,12},{10,14},{12,0},{14,2},{1,5},{3,7},... | collective-permute-start | bytes 786440 | tf_op jit(solution)/shard_map/ppermute | solution.py:100
  226.8 20.9 %collective-permute-start.3 = (bf16[64,2048]{1,0:T(8,128)(2,1)S(1)}, bf16[64,2048]{1,0:T(8,128)(2,1)S(1)}, u32[]{:S(2)}, u32[]{:S(2)}) collective-permute-start(bf16[64,2048]{1,0:T(8,128)(2,1)S(1)} %get-tuple-element.22), channel_id=1, source_target_pairs={{0,8},{2,10},{4,12},{6,14},{8,0},{10,2},{12,4},{14,6},{1,9},{3,11}... | collective-permute-start | bytes 786440 | tf_op jit(solution)/shard_map/ppermute | solution.py:100
  227.9 23.7 %collective-permute-start.4 = (bf16[64,2048]{1,0:T(8,128)(2,1)S(1)}, bf16[64,2048]{1,0:T(8,128)(2,1)S(1)}, u32[]{:S(2)}, u32[]{:S(2)}) collective-permute-start(bf16[64,2048]{1,0:T(8,128)(2,1)S(1)} %get-tuple-element.21), channel_id=1, source_target_pairs={{0,12},{2,14},{4,0},{6,2},{8,4},{10,6},{12,8},{14,10},{1,13},{3,15... | collective-permute-start | bytes 786440 | tf_op jit(solution)/shard_map/ppermute | solution.py:100
  229.3 23.0 %collective-permute-start.11 = (bf16[64,2048]{1,0:T(8,128)(2,1)S(1)}, bf16[64,2048]{1,0:T(8,128)(2,1)S(1)}, u32[]{:S(2)}, u32[]{:S(2)}) collective-permute-start(bf16[64,2048]{1,0:T(8,128)(2,1)S(1)} %fusion.25), channel_id=1, source_target_pairs={{0,1},{1,0},{2,3},{3,2},{4,5},{5,4},{6,7},{7,6},{8,9},{9,8},{10,11... | collective-permute-start | bytes 786440 | tf_op jit(solution)/shard_map/ppermute | solution.py:90
  251.7 2.2 collective-permute-start.5
  252.3 2.5 copy-start.1

commit v3 on v2

--- a/solution.py
+++ b/solution.py
@@ -106,12 +106,15 @@
     return jnp.where(axis_index == 0, jnp.stack([first, second]), jnp.stack([second, first]))
 
 
-def scatter_tokens(partial, rows):
-    width = partial.shape[1]
+def core_sum(partial, rows):
     outer = lax.axis_size("fs") // 2
-    blocks = partial.reshape(2, 2, outer, rows // 2, width)
+    blocks = partial.astype(jnp.bfloat16).reshape(2, 2, outer, rows // 2, partial.shape[1])
     got = swap(blocks[1], "tp")
-    blocks = (blocks[0].astype(jnp.float32) + got.astype(jnp.float32)).astype(jnp.bfloat16)
+    return (blocks[0].astype(jnp.float32) + got.astype(jnp.float32)).astype(jnp.bfloat16)
+
+
+def scatter_tokens(blocks):
+    outer = lax.axis_size("fs") // 2
     got = swap(blocks[1], "fs")
     blocks = (blocks[0].astype(jnp.float32) + got.astype(jnp.float32)).astype(jnp.bfloat16)
     place = lax.axis_index("fs") // 2
@@ -121,7 +124,7 @@
         total = total + line_shift(sent, s).astype(jnp.float32)
     half = total.astype(jnp.bfloat16)
     whole = ordered(half, swap(half, "tp"), lax.axis_index("tp"))
-    return whole.reshape(rows, width).astype(jnp.float32)
+    return whole.reshape(-1, half.shape[1]).astype(jnp.float32)
 
 
 def gather_kernel(
@@ -324,6 +327,34 @@
     return tok, up_own.reshape(n_fs * depth, own_units), down_own
 
 
+def add_kernel(own, got, total, out):
+    first = lax.axis_index("rep") == 0
+    parts, _, part = own.shape
+    for k in range(parts):
+        mine, other = own[k].astype(jnp.float32), got[k].astype(jnp.float32)
+        left = slice(2 * k * part, (2 * k + 1) * part)
+        right = slice((2 * k + 1) * part, (2 * k + 2) * part)
+        out[:, left] = total[:, left] + jnp.where(first, mine, other)
+        out[:, right] = total[:, right] + jnp.where(first, other, mine)
+
+
+def add_up(own, got, total):
+    parts, depth, part = own.shape
+    rows = depth // 4
+    blocks = pl.BlockSpec((parts, rows, part), lambda i: (0, i, 0))
+    whole = pl.BlockSpec((rows, total.shape[1]), lambda i: (i, 0))
+    return pl.pallas_call(
+        add_kernel,
+        grid=(4,),
+        out_shape=jax.ShapeDtypeStruct(total.shape, total.dtype),
+        in_specs=[blocks, blocks, whole],
+        out_specs=whole,
+        cost_estimate=pl.CostEstimate(
+            flops=2 * total.size, bytes_accessed=10 * total.size, transcendentals=0
+        ),
+    )(own, got, total)
+
+
 def hidden_body(
     x_later, kept_input_rows, cotangent, norm_gain_vector, up_weight, down_weight, up_sum, down_sum
 ):
@@ -353,6 +384,16 @@
     hidden_saved = squared_relu(pre_saved)
     hidden_grad = lax.dot_general(cot, down_own, TRANSPOSED, preferred_element_type=jnp.float32)
     pre_grad = (hidden_grad * 2.0 * jax.nn.relu(pre_saved)).astype(jnp.bfloat16)
+    back_part = lax.dot_general(pre_grad, up_own, TRANSPOSED, preferred_element_type=jnp.float32)
+    back_blocks = core_sum(back_part, row_count)
+    hidden_later = squared_relu(
+        jnp.dot(normed_next, up_own, preferred_element_type=jnp.float32)
+    )
+    mixed_part = jnp.dot(hidden_later, down_own, preferred_element_type=jnp.float32)
+    mixed_blocks = core_sum(mixed_part, row_count)
+    pre_grad, hidden_saved, mixed_blocks = lax.optimization_barrier(
+        (pre_grad, hidden_saved, mixed_blocks)
+    )
     up_grad = grad_scale * lax.dot_general(
         normed_saved, pre_grad, LEADING, preferred_element_type=jnp.float32
     )
@@ -361,23 +402,17 @@
     )
     up_got = swap(up_grad[:, part:].astype(jnp.bfloat16), "rep")
     down_got = swap(down_grad[part:].astype(jnp.bfloat16), "rep")
-    back_part = lax.dot_general(pre_grad, up_own, TRANSPOSED, preferred_element_type=jnp.float32)
-    hidden_later = squared_relu(
-        jnp.dot(normed_next, up_own, preferred_element_type=jnp.float32)
-    )
-    mixed_part = jnp.dot(hidden_later, down_own, preferred_element_type=jnp.float32)
     up_half = (up_grad[:, :part] + up_got.astype(jnp.float32)).astype(jnp.bfloat16)
     down_half = (down_grad[:part] + down_got.astype(jnp.float32)).astype(jnp.bfloat16)
     up_half = lax.all_to_all(up_half.reshape(n_fs, depth, part), "fs", 0, 0, tiled=True)
     down_half = down_half.reshape(part, n_fs, depth).transpose(1, 0, 2)
     down_half = lax.all_to_all(down_half, "fs", 0, 0, tiled=True)
-    up_added = ordered(up_half, swap(up_half, "rep"), group)
-    up_added = up_added.transpose(2, 1, 0, 3).reshape(depth, units)
+    up_total = add_up(up_half, swap(up_half, "rep"), up_sum)
     down_added = ordered(down_half, swap(down_half, "rep"), group)
     down_added = down_added.transpose(1, 0, 2, 3).reshape(units, depth)
 
-    back_sum = scatter_tokens(back_part.astype(jnp.bfloat16), row_count)
-    mixed = scatter_tokens(mixed_part.astype(jnp.bfloat16), row_count).astype(jnp.bfloat16)
+    back_sum = scatter_tokens(back_blocks)
+    mixed = scatter_tokens(mixed_blocks).astype(jnp.bfloat16)
     scaled_rows = back_sum * norm_gain_vector
     input_gradient_rows = (
         inverse_rms_kept
@@ -389,7 +424,7 @@
     return (
         mixed,
         input_gradient_rows,
-        up_sum + up_added.astype(jnp.float32),
+        up_total,
         down_sum + down_added.astype(jnp.float32),
     )
 
@@ -398,7 +433,7 @@
     units = args[4].shape[1]
     n_fs = lax.axis_size("fs")
     pairs = lax.axis_size("tp") == 2 and lax.axis_size("rep") == 2 and n_fs % 2 == 0
-    return (hidden_body if pairs and units % (128 * n_fs) == 0 else body)(*args)
+    return (hidden_body if pairs and units % (256 * n_fs) == 0 else body)(*args)
 
 
 def solution(mesh):

time: 255 us -> 273 us (1.071)
  starting transfers between devices: 43.4 us -> 64.9 us
  waiting for transfers between devices: 56.2 us -> 48.5 us
  Pallas kernels: 87.3 us -> 91.3 us
    ppermute x6, starting transfers between devices: 9 us -> 34.5 us  [line_shift(): lax.ppermute(values, 'fs', [(i, (i // 2 + shift) % outer * 2 + i % 2) for...]
    ppermute x10, waiting for transfers between devices: 33.2 us -> 23.8 us  [swap(): return lax.ppermute(values, axis, [(i, i ^ 1) for i in range(size)])]
    convert_element_type x2 -> x0, local copies, waits for them, and re-layouts: 6.82 us -> none  [hidden_body(): up_added.astype(jnp.float32)]
    ppermute x6, waiting for transfers between devices: 19.2 us -> 24.7 us  [line_shift(): lax.ppermute(values, 'fs', [(i, (i // 2 + shift) % outer * 2 + i % 2) for...]
    convert_element_type x1 -> x2, other arithmetic: 0.19 us -> 5.53 us  [core_sum(): (blocks[0].astype(jnp.float32) + got.astype(jnp.float32)).astype(jnp.bflo...]
    convert_element_type x4 -> x2, other arithmetic: 7.97 us -> 3.22 us  [scatter_tokens(): (blocks[0].astype(jnp.float32) + got.astype(jnp.float32)).astype(jnp.bflo...]
    unnamed x22 -> x44, local copies, waits for them, and re-layouts: 1 us -> 5.14 us
    pallas_call x0 -> x1, Pallas kernels: none -> 4.07 us  [add_up(): pl.pallas_call(add_kernel, grid=(4,), out_shape=jax.ShapeDtypeStruct(tota...]
  transfers between devices with their start and end apart: 18 -> 18, of which waited for: 7 -> 6; matrix products, arithmetic and copies ran while one was open for 20% -> 12% of each run, Pallas kernels for 0% -> 0%
where the time goes in v3:
time: 273 us; the launch traced here: 272 us
  Pallas kernels  91.3 us (33%)
  starting transfers between devices  64.9 us (24%)
  waiting for transfers between devices  48.5 us (18%)
  local copies, waits for them, and re-layouts  27 us (10%)
  other arithmetic  23.8 us (9%)
  matrix products  15 us (5%)
    pallas_call x1, Pallas kernels, gather_all(): pl.pallas_call(functools.partial(gather_kernel, n_fs), out_shape=(jax.Sha...  87.3 us
    ppermute x6, starting transfers between devices, line_shift(): lax.ppermute(values, 'fs', [(i, (i // 2 + shift) % outer * 2 + i % 2) for...  34.5 us
    ppermute x6, waiting for transfers between devices, line_shift(): lax.ppermute(values, 'fs', [(i, (i // 2 + shift) % outer * 2 + i % 2) for...  24.7 us
    ppermute x10, waiting for transfers between devices, swap(): return lax.ppermute(values, axis, [(i, i ^ 1) for i in range(size)])  23.8 us
    all_to_all x1, starting transfers between devices, hidden_body(): down_half = lax.all_to_all(down_half, 'fs', 0, 0, tiled=True)  17.5 us
    ppermute x10, starting transfers between devices, swap(): return lax.ppermute(values, axis, [(i, i ^ 1) for i in range(size)])  9.15 us
    slice x1, local copies, waits for them, and re-layouts, hidden_body(): tok[i].reshape(-1, width)  9.12 us
    dot_general x1, matrix products, hidden_body(): jnp.dot(hidden_later, down_own, preferred_element_type=jnp.float32)  8.52 us
  transfers between devices with their start and end apart: 18, of which 6 were waited for; matrix products, arithmetic and copies ran while one was open for 12% of the time, Pallas kernels for 0%

profile of v3, /device:TPU:11, one launch (start us, length us, event | category | flops | bytes accessed | tf_op | source)
XLA Modules:
  0.0 271.5 jit_solution(10458726563773835303)
XLA Ops:
  0.7 1.3 fusion.16
  1.9 1.2 fusion.17
  3.2 1.5 fusion.11
  4.8 1.0 pad_maximum_fusion.own
  5.8 87.3 %shard_map.111 = (bf16[3,2,2,4,64,2048]{5,4,3,2,1,0:T(8,128)(2,1)}, bf16[8,256,256]{2,1,0:T(8,128)(2,1)}, bf16[256,2048]{1,0:T(8,128)(2,1)}) custom-call(bf16[3,64,2048]{2,1,0:T(8,128)(2,1)} %pad_maximum_fusion.own, bf16[256,2048]{1,0:T(8,128)(2,1)} %up.1, bf16[2048,256]{1,0:T(8,128)(2,1)} %down.1), custom_call_target="tpu_custom_call" | custom-call | tf_op jit(solution)/shard_map/pallas_call | solution.py:312
  93.1 9.1 %fusion.31 = (bf16[1,2,2,4,64,2048]{5,4,3,2,1,0:T(8,128)(2,1)}, bf16[1,2,2,4,64,2048]{5,4,3,2,1,0:T(8,128)(2,1)}, bf16[1,2,2,4,64,2048]{5,4,3,2,1,0:T(8,128)(2,1)}) fusion(bf16[3,2,2,4,64,2048]{5,4,3,2,1,0:T(8,128)(2,1)} %get-tuple-element.10), kind=kLoop, calls=%fused_computation.75 | loop fusion | bytes 25165824 | tf_op jit(solution)/shard_map/slice | solution.py:381
  102.2 8.5 %convolution_convert_fusion.1 = bf16[1024,2048]{1,0:T(8,128)(2,1)} fusion(bf16[256,2048]{1,0:T(8,128)(2,1)S(1)} %copy-done.20, bf16[1024,2048]{1,0:T(8,128)(2,1)} %bitcast.86, bf16[2048,256]{1,0:T(8,128)(2,1)S(1)} %bitcast.91), kind=kOutput, calls=%fused_computation.5 | convolution fusion | flops 2150367232 | bytes 10485760 | tf_op jit(solution)/shard_map/dot_general | solution.py:392
  110.7 5.0 %fusion.33 = (bf16[512,2048]{1,0:T(8,128)(2,1)}, bf16[512,2048]{1,0:T(8,128)(2,1)}) fusion(bf16[1024,2048]{1,0:T(8,128)(2,1)} %convolution_convert_fusion.1), kind=kLoop, calls=%fused_computation.77 | loop fusion | bytes 8388608 | tf_op jit(solution)/shard_map/slice | solution.py:112
  115.7 0.1 collective-permute-start
  115.9 1.3 multiply_convert_fusion
  117.1 0.9 copy-done.10
  118.0 0.3 copy-done.21
  118.3 1.3 fusion.9
  119.6 1.3 convolution_convert_fusion
  120.9 2.5 fusion.32
  123.4 0.4 collective-permute-start.6
  123.8 1.3 copy-done.13
  125.1 3.2 %fusion.1 = bf16[2,4,64,2048]{3,2,1,0:T(8,128)(2,1)S(1)} fusion(bf16[2,4,64,2048]{3,2,1,0:T(8,128)(2,1)} %bitcast.81, bf16[2,4,64,2048]{3,2,1,0:T(8,128)(2,1)} %copy-done.13), kind=kLoop, calls=%fused_computation.3 | loop fusion | flops 4194304 | bytes 6291456 | tf_op jit(solution)/shard_map/convert_element_type | solution.py:113
  128.3 0.3 copy-done.11
  128.6 1.3 convolution_multiply_fusion
  129.9 0.3 collective-permute-start.14
  130.2 0.5 copy-done.9
  130.8 1.4 convolution_multiply_fusion.1
  132.2 1.0 slice.91
  133.1 0.7 collective-permute-start.12
  133.8 2.4 fusion
  136.2 1.2 slice_bitcast_fusion
  137.4 1.2 collective-permute-start.7
  138.6 1.1 slice_bitcast_fusion.2
  139.6 0.3 collective-permute-start.1
  139.9 3.5 %collective-permute-done.14 = bf16[128,2048]{1,0:T(8,128)(2,1)S(1)} collective-permute-done((bf16[128,2048]{1,0:T(8,128)(2,1)S(1)}, bf16[128,2048]{1,0:T(8,128)(2,1)S(1)}, u32[]{:S(2)}, u32[]{:S(2)}) %collective-permute-start.14) | collective-permute-done | bytes 524320 | tf_op jit(solution)/shard_map/ppermute | solution.py:90
  143.5 0.1 fusion.20
  143.6 0.8 copy.17
  144.4 17.5 %all-to-all-start.1 = ((bf16[8,128,256]{2,1,0:T(8,128)(2,1)}), bf16[8,128,256]{2,1,0:T(8,128)(2,1)S(1)}, u32[]{:S(2)}, u32[]{:S(2)}) async-start(bf16[8,128,256]{2,1,0:T(8,128)(2,1)} %bitcast.78), calls=%async_computation.1 | async-start | bytes 1048576 | tf_op jit(solution)/shard_map/all_to_all | solution.py:409
  161.9 2.4 fusion.21
  164.3 1.6 fusion.2
  166.0 1.0 dynamic-slice_bitcast_fusion.2
  167.0 14.8 %collective-permute-start.10 = (bf16[64,2048]{1,0:T(8,128)(2,1)}, bf16[64,2048]{1,0:T(8,128)(2,1)S(1)}, u32[]{:S(2)}, u32[]{:S(2)}) collective-permute-start(bf16[64,2048]{1,0:T(8,128)(2,1)} %get-tuple-element.24), channel_id=1, source_target_pairs={{0,12},{2,14},{4,0},{6,2},{8,4},{10,6},{12,8},{14,10},{1,13},{3,15... | collective-permute-start | bytes 786440 | tf_op jit(solution)/shard_map/ppermute | solution.py:100
  181.8 4.2 %collective-permute-start.9 = (bf16[64,2048]{1,0:T(8,128)(2,1)}, bf16[64,2048]{1,0:T(8,128)(2,1)}, u32[]{:S(2)}, u32[]{:S(2)}) collective-permute-start(bf16[64,2048]{1,0:T(8,128)(2,1)} %get-tuple-element.25), channel_id=1, source_target_pairs={{0,8},{2,10},{4,12},{6,14},{8,0},{10,2},{12,4},{14,6},{1,9},{3,11}... | collective-permute-start | bytes 786440 | tf_op jit(solution)/shard_map/ppermute | solution.py:100
  186.0 2.4 collective-permute-done.1
  188.4 1.6 fusion.3
  190.1 0.9 copy-done.7
  191.0 0.3 collective-permute-start.2
  191.3 15.0 %collective-permute-start.3 = (bf16[64,2048]{1,0:T(8,128)(2,1)S(1)}, bf16[64,2048]{1,0:T(8,128)(2,1)S(1)}, u32[]{:S(2)}, u32[]{:S(2)}) collective-permute-start(bf16[64,2048]{1,0:T(8,128)(2,1)S(1)} %get-tuple-element.28), channel_id=1, source_target_pairs={{0,8},{2,10},{4,12},{6,14},{8,0},{10,2},{12,4},{14,6},{1,9},{3,11}... | collective-permute-start | bytes 786440 | tf_op jit(solution)/shard_map/ppermute | solution.py:100
  206.3 3.7 %all-to-all-start = ((bf16[8,256,128]{2,1,0:T(8,128)(2,1)}), bf16[8,256,128]{2,1,0:T(8,128)(2,1)S(1)}, u32[]{:S(2)}, u32[]{:S(2)}) async-start(bf16[8,256,128]{2,1,0:T(8,128)(2,1)} %bitcast.29), calls=%async_computation | async-start | bytes 1048576 | tf_op jit(solution)/shard_map/all_to_all | solution.py:407
  210.1 0.2 collective-permute-start.4
  210.3 1.2 fusion.25
  211.5 3.3 %collective-permute-start.11 = (bf16[64,2048]{1,0:T(8,128)(2,1)S(1)}, bf16[64,2048]{1,0:T(8,128)(2,1)S(1)}, u32[]{:S(2)}, u32[]{:S(2)}) collective-permute-start(bf16[64,2048]{1,0:T(8,128)(2,1)S(1)} %fusion.25), channel_id=1, source_target_pairs={{0,1},{1,0},{2,3},{3,2},{4,5},{5,4},{6,7},{7,6},{8,9},{9,8},{10,11... | collective-permute-start | bytes 786440 | tf_op jit(solution)/shard_map/ppermute | solution.py:90
  214.8 16.3 %collective-permute-done.3 = bf16[64,2048]{1,0:T(8,128)(2,1)S(1)} collective-permute-done((bf16[64,2048]{1,0:T(8,128)(2,1)S(1)}, bf16[64,2048]{1,0:T(8,128)(2,1)S(1)}, u32[]{:S(2)}, u32[]{:S(2)}) %collective-permute-start.3) | collective-permute-done | bytes 262176 | tf_op jit(solution)/shard_map/ppermute | solution.py:100
  231.1 8.4 %collective-permute-done.4 = bf16[64,2048]{1,0:T(8,128)(2,1)S(1)} collective-permute-done((bf16[64,2048]{1,0:T(8,128)(2,1)S(1)}, bf16[64,2048]{1,0:T(8,128)(2,1)S(1)}, u32[]{:S(2)}, u32[]{:S(2)}) %collective-permute-start.4) | collective-permute-done | bytes 262176 | tf_op jit(solution)/shard_map/ppermute | solution.py:100
  239.5 1.1 fusion.28
  240.6 1.4 collective-permute-start.5
  242.0 1.1 collective-permute-start.15
  243.0 0.4 collective-permute-start.13
  243.4 0.1 maximum_select_fusion.2
  243.6 0.3 fusion.12
  243.9 1.9 maximum_select_fusion.1
  245.8 1.2 fusion.15
  247.0 8.4 %collective-permute-done.15 = bf16[8,128,256]{2,1,0:T(8,128)(2,1)S(1)} collective-permute-done((bf16[8,128,256]{2,1,0:T(8,128)(2,1)S(1)}, bf16[8,128,256]{2,1,0:T(8,128)(2,1)S(1)}, u32[]{:S(2)}, u32[]{:S(2)}) %collective-permute-start.15) | collective-permute-done | bytes 524320 | tf_op jit(solution)/shard_map/ppermute | solution.py:90
  255.4 0.1 fusion.22
  255.5 1.6 bitcast_add_fusion
  257.1 9.5 %collective-permute-done.13.got = bf16[8,256,128]{2,1,0:T(8,128)(2,1)S(1)} collective-permute-done((bf16[8,256,128]{2,1,0:T(8,128)(2,1)S(1)}, bf16[8,256,128]{2,1,0:T(8,128)(2,1)S(1)}, u32[]{:S(2)}, u32[]{:S(2)}) %collective-permute-start.13) | collective-permute-done | bytes 524320 | tf_op jit(solution)/shard_map/ppermute | solution.py:90
  266.6 0.8 copy-done.18
  267.4 4.1 %shard_map.112 = f32[256,2048]{1,0:T(8,128)} custom-call(bf16[8,256,128]{2,1,0:T(8,128)(2,1)} %copy-done.14, bf16[8,256,128]{2,1,0:T(8,128)(2,1)} %copy-done.18, f32[256,2048]{1,0:T(8,128)} %total.1), custom_call_target="tpu_custom_call" | custom-call | flops 1048576 | bytes 5242880 | tf_op jit(solution)/shard_map/pallas_call | solution.py:346
  (57 shorter events, 0.4 us)
Async XLA Ops:
  0.6 4.2 %copy-start = (bf16[128,2048]{1,0:T(8,128)(2,1)S(1)}, bf16[128,2048]{1,0:T(8,128)(2,1)}, u32[]{:S(2)}) copy-start(bf16[128,2048]{1,0:T(8,128)(2,1)} %param.10) | copy-start | bytes 1572868
  93.1 9.1 %copy-start.16 = (bf16[8,256,256]{2,1,0:T(8,128)(2,1)S(1)}, bf16[8,256,256]{2,1,0:T(8,128)(2,1)}, u32[]{:S(2)}) copy-start(bf16[8,256,256]{2,1,0:T(8,128)(2,1)} %get-tuple-element.12) | copy-start | bytes 3145732
  93.1 9.1 %copy-start.20 = (bf16[256,2048]{1,0:T(8,128)(2,1)S(1)}, bf16[256,2048]{1,0:T(8,128)(2,1)}, u32[]{:S(2)}) copy-start(bf16[256,2048]{1,0:T(8,128)(2,1)} %get-tuple-element.11) | copy-start | bytes 3145732
  110.7 5.1 %copy-start.8 = (bf16[1,2,2,4,64,2048]{5,4,3,2,1,0:T(8,128)(2,1)S(1)}, bf16[1,2,2,4,64,2048]{5,4,3,2,1,0:T(8,128)(2,1)}, u32[]{:S(2)}) copy-start(bf16[1,2,2,4,64,2048]{5,4,3,2,1,0:T(8,128)(2,1)} %get-tuple-element.17) | copy-start | bytes 12582916
  110.7 5.1 %copy-start.17 = (bf16[8,256,256]{2,1,0:T(8,128)(2,1)S(1)}, bf16[8,256,256]{2,1,0:T(8,128)(2,1)}, u32[]{:S(2)}) copy-start(bf16[8,256,256]{2,1,0:T(8,128)(2,1)} %get-tuple-element.12) | copy-start | bytes 3145732
  115.7 8.1 %collective-permute-start = (bf16[2,4,64,2048]{3,2,1,0:T(8,128)(2,1)}, bf16[2,4,64,2048]{3,2,1,0:T(8,128)(2,1)S(1)}, u32[]{:S(2)}, u32[]{:S(2)}) collective-permute-start(bf16[2,4,64,2048]{3,2,1,0:T(8,128)(2,1)} %bitcast.8), channel_id=1, source_target_pairs={{0,1},{1,0},{2,3},{3,2},{4,5},{5,4},{6,7},{7,6},{8,9},{9,8},{10,11... | collective-permute-start | bytes 6291464 | tf_op jit(solution)/shard_map/ppermute | solution.py:90
  115.8 2.2 copy-start.10
  115.8 2.5 copy-start.21
  123.4 10.4 %collective-permute-start.6 = (bf16[2,4,64,2048]{3,2,1,0:T(8,128)(2,1)}, bf16[2,4,64,2048]{3,2,1,0:T(8,128)(2,1)}, u32[]{:S(2)}, u32[]{:S(2)}) collective-permute-start(bf16[2,4,64,2048]{3,2,1,0:T(8,128)(2,1)} %bitcast.19), channel_id=1, source_target_pairs={{0,1},{1,0},{2,3},{3,2},{4,5},{5,4},{6,7},{7,6},{8,9},{9,8},{10,11... | collective-permute-start | bytes 6291464 | tf_op jit(solution)/shard_map/ppermute | solution.py:90
  123.8 1.3 copy-start.13
  125.1 3.4 %copy-start.11 = (bf16[1,2,2,4,64,2048]{5,4,3,2,1,0:T(8,128)(2,1)S(1)}, bf16[1,2,2,4,64,2048]{5,4,3,2,1,0:T(8,128)(2,1)}, u32[]{:S(2)}) copy-start(bf16[1,2,2,4,64,2048]{5,4,3,2,1,0:T(8,128)(2,1)} %get-tuple-element.18) | copy-start | bytes 12582916
  128.6 2.2 copy-start.9
  129.9 13.5 %collective-permute-start.14 = (bf16[128,2048]{1,0:T(8,128)(2,1)S(1)}, bf16[128,2048]{1,0:T(8,128)(2,1)S(1)}, u32[]{:S(2)}, u32[]{:S(2)}) collective-permute-start(bf16[128,2048]{1,0:T(8,128)(2,1)S(1)} %slice.90), channel_id=1, source_target_pairs={{0,16},{16,0},{1,17},{17,1},{2,18},{18,2},{3,19},{19,3},{4,20},{20... | collective-permute-start | bytes 1572872 | tf_op jit(solution)/shard_map/ppermute | solution.py:90
  130.8 3.1 %copy-start.4 = (bf16[512,2048]{1,0:T(8,128)(2,1)S(1)}, bf16[512,2048]{1,0:T(8,128)(2,1)}, u32[]{:S(2)}) copy-start(bf16[512,2048]{1,0:T(8,128)(2,1)} %get-tuple-element.20) | copy-start | bytes 6291460
  132.2 1.7 copy-start.15
  133.1 28.8 %collective-permute-start.12 = (bf16[2048,128]{1,0:T(8,128)(2,1)}, bf16[2048,128]{1,0:T(8,128)(2,1)}, u32[]{:S(2)}, u32[]{:S(2)}) collective-permute-start(bf16[2048,128]{1,0:T(8,128)(2,1)} %slice.91), channel_id=1, source_target_pairs={{0,16},{16,0},{1,17},{17,1},{2,18},{18,2},{3,19},{19,3},{4,20},{20... | collective-permute-start | bytes 1572872 | tf_op jit(solution)/shard_map/ppermute | solution.py:90
  136.2 3.4 %copy-start.2 = (bf16[2,4,64,2048]{3,2,1,0:T(8,128)(2,1)}, bf16[2,4,64,2048]{3,2,1,0:T(8,128)(2,1)S(1)}, u32[]{:S(2)}) copy-start(bf16[2,4,64,2048]{3,2,1,0:T(8,128)(2,1)S(1)} %fusion) | copy-start | bytes 6291460
  137.4 27.0 %collective-permute-start.7 = (bf16[4,64,2048]{2,1,0:T(8,128)(2,1)}, bf16[4,64,2048]{2,1,0:T(8,128)(2,1)}, u32[]{:S(2)}, u32[]{:S(2)}) collective-permute-start(bf16[4,64,2048]{2,1,0:T(8,128)(2,1)} %slice_bitcast_fusion), channel_id=1, source_target_pairs={{0,2},{2,0},{4,6},{6,4},{8,10},{10,8},{12,14},{14,12},{1,3},{3,1},... | collective-permute-start | bytes 3145736 | tf_op jit(solution)/shard_map/ppermute | solution.py:90
  139.6 48.8 %collective-permute-start.1 = (bf16[4,64,2048]{2,1,0:T(8,128)(2,1)}, bf16[4,64,2048]{2,1,0:T(8,128)(2,1)}, u32[]{:S(2)}, u32[]{:S(2)}) collective-permute-start(bf16[4,64,2048]{2,1,0:T(8,128)(2,1)} %slice_bitcast_fusion.2), channel_id=1, source_target_pairs={{0,2},{2,0},{4,6},{6,4},{8,10},{10,8},{12,14},{14,12},{1,3},{3,1},... | collective-permute-start | bytes 3145736 | tf_op jit(solution)/shard_map/ppermute | solution.py:90
  144.4 61.9 %all-to-all-start.1 = ((bf16[8,128,256]{2,1,0:T(8,128)(2,1)}), bf16[8,128,256]{2,1,0:T(8,128)(2,1)S(1)}, u32[]{:S(2)}, u32[]{:S(2)}) async-start(bf16[8,128,256]{2,1,0:T(8,128)(2,1)} %bitcast.78), calls=%async_computation.1 | async-start | bytes 1048576 | tf_op jit(solution)/shard_map/all_to_all | solution.py:409
  161.9 2.4 copy-start.3
  166.0 24.1 %copy-start.6 = (bf16[4,64,2048]{2,1,0:T(8,128)(2,1)}, bf16[4,64,2048]{2,1,0:T(8,128)(2,1)S(1)}, u32[]{:S(2)}) copy-start(bf16[4,64,2048]{2,1,0:T(8,128)(2,1)S(1)} %fusion.2) | copy-start | bytes 3145732
  167.0 43.1 %collective-permute-start.10 = (bf16[64,2048]{1,0:T(8,128)(2,1)}, bf16[64,2048]{1,0:T(8,128)(2,1)S(1)}, u32[]{:S(2)}, u32[]{:S(2)}) collective-permute-start(bf16[64,2048]{1,0:T(8,128)(2,1)} %get-tuple-element.24), channel_id=1, source_target_pairs={{0,12},{2,14},{4,0},{6,2},{8,4},{10,6},{12,8},{14,10},{1,13},{3,15... | collective-permute-start | bytes 786440 | tf_op jit(solution)/shard_map/ppermute | solution.py:100
  181.8 28.5 %collective-permute-start.8 = (bf16[64,2048]{1,0:T(8,128)(2,1)}, bf16[64,2048]{1,0:T(8,128)(2,1)}, u32[]{:S(2)}, u32[]{:S(2)}) collective-permute-start(bf16[64,2048]{1,0:T(8,128)(2,1)} %get-tuple-element.23), channel_id=1, source_target_pairs={{0,4},{2,6},{4,8},{6,10},{8,12},{10,14},{12,0},{14,2},{1,5},{3,7},... | collective-permute-start | bytes 786440 | tf_op jit(solution)/shard_map/ppermute | solution.py:100
  181.8 28.5 %collective-permute-start.9 = (bf16[64,2048]{1,0:T(8,128)(2,1)}, bf16[64,2048]{1,0:T(8,128)(2,1)}, u32[]{:S(2)}, u32[]{:S(2)}) collective-permute-start(bf16[64,2048]{1,0:T(8,128)(2,1)} %get-tuple-element.25), channel_id=1, source_target_pairs={{0,8},{2,10},{4,12},{6,14},{8,0},{10,2},{12,4},{14,6},{1,9},{3,11}... | collective-permute-start | bytes 786440 | tf_op jit(solution)/shard_map/ppermute | solution.py:100
  190.0 1.0 copy-start.7
  191.0 23.8 %collective-permute-start.2 = (bf16[64,2048]{1,0:T(8,128)(2,1)S(1)}, bf16[64,2048]{1,0:T(8,128)(2,1)S(1)}, u32[]{:S(2)}, u32[]{:S(2)}) collective-permute-start(bf16[64,2048]{1,0:T(8,128)(2,1)S(1)} %get-tuple-element.26), channel_id=1, source_target_pairs={{0,4},{2,6},{4,8},{6,10},{8,12},{10,14},{12,0},{14,2},{1,5},{3,7},... | collective-permute-start | bytes 786440 | tf_op jit(solution)/shard_map/ppermute | solution.py:100
  191.3 39.8 %collective-permute-start.3 = (bf16[64,2048]{1,0:T(8,128)(2,1)S(1)}, bf16[64,2048]{1,0:T(8,128)(2,1)S(1)}, u32[]{:S(2)}, u32[]{:S(2)}) collective-permute-start(bf16[64,2048]{1,0:T(8,128)(2,1)S(1)} %get-tuple-element.28), channel_id=1, source_target_pairs={{0,8},{2,10},{4,12},{6,14},{8,0},{10,2},{12,4},{14,6},{1,9},{3,11}... | collective-permute-start | bytes 786440 | tf_op jit(solution)/shard_map/ppermute | solution.py:100
  206.3 36.7 %all-to-all-start = ((bf16[8,256,128]{2,1,0:T(8,128)(2,1)}), bf16[8,256,128]{2,1,0:T(8,128)(2,1)S(1)}, u32[]{:S(2)}, u32[]{:S(2)}) async-start(bf16[8,256,128]{2,1,0:T(8,128)(2,1)} %bitcast.29), calls=%async_computation | async-start | bytes 1048576 | tf_op jit(solution)/shard_map/all_to_all | solution.py:407
  210.1 33.5 %copy-start.5 = (bf16[128,2048]{1,0:T(8,128)(2,1)S(1)}, bf16[128,2048]{1,0:T(8,128)(2,1)}, u32[]{:S(2)}) copy-start(bf16[128,2048]{1,0:T(8,128)(2,1)} %param.9) | copy-start | bytes 1572868
  210.1 33.5 %copy-start.19 = (f32[2048]{0:T(1024)S(1)}, f32[2048]{0:T(1024)}, u32[]{:S(2)}) copy-start(f32[2048]{0:T(1024)} %param.11) | copy-start | bytes 24580
  210.1 29.4 %collective-permute-start.4 = (bf16[64,2048]{1,0:T(8,128)(2,1)S(1)}, bf16[64,2048]{1,0:T(8,128)(2,1)S(1)}, u32[]{:S(2)}, u32[]{:S(2)}) collective-permute-start(bf16[64,2048]{1,0:T(8,128)(2,1)S(1)} %get-tuple-element.27), channel_id=1, source_target_pairs={{0,12},{2,14},{4,0},{6,2},{8,4},{10,6},{12,8},{14,10},{1,13},{3,15... | collective-permute-start | bytes 786440 | tf_op jit(solution)/shard_map/ppermute | solution.py:100
  211.5 31.9 %collective-permute-start.11 = (bf16[64,2048]{1,0:T(8,128)(2,1)S(1)}, bf16[64,2048]{1,0:T(8,128)(2,1)S(1)}, u32[]{:S(2)}, u32[]{:S(2)}) collective-permute-start(bf16[64,2048]{1,0:T(8,128)(2,1)S(1)} %fusion.25), channel_id=1, source_target_pairs={{0,1},{1,0},{2,3},{3,2},{4,5},{5,4},{6,7},{7,6},{8,9},{9,8},{10,11... | collective-permute-start | bytes 786440 | tf_op jit(solution)/shard_map/ppermute | solution.py:90
  240.6 3.3 %collective-permute-start.5 = (bf16[64,2048]{1,0:T(8,128)(2,1)S(1)}, bf16[64,2048]{1,0:T(8,128)(2,1)}, u32[]{:S(2)}, u32[]{:S(2)}) collective-permute-start(bf16[64,2048]{1,0:T(8,128)(2,1)S(1)} %fusion.28), channel_id=1, source_target_pairs={{0,1},{1,0},{2,3},{3,2},{4,5},{5,4},{6,7},{7,6},{8,9},{9,8},{10,11... | collective-permute-start | bytes 786440 | tf_op jit(solution)/shard_map/ppermute | solution.py:90
  242.0 13.4 %collective-permute-start.15 = (bf16[8,128,256]{2,1,0:T(8,128)(2,1)S(1)}, bf16[8,128,256]{2,1,0:T(8,128)(2,1)S(1)}, u32[]{:S(2)}, u32[]{:S(2)}) collective-permute-start(bf16[8,128,256]{2,1,0:T(8,128)(2,1)S(1)} %all-to-all-done.1), channel_id=1, source_target_pairs={{0,16},{16,0},{1,17},{17,1},{2,18},{18,2},{3,19},{19,3},{4,20},{20... | collective-permute-start | bytes 1572872 | tf_op jit(solution)/shard_map/ppermute | solution.py:90
  243.0 3.9 %copy-start.14 = (bf16[8,256,128]{2,1,0:T(8,128)(2,1)}, bf16[8,256,128]{2,1,0:T(8,128)(2,1)S(1)}, u32[]{:S(2)}) copy-start(bf16[8,256,128]{2,1,0:T(8,128)(2,1)S(1)} %all-to-all-done.own) | copy-start | bytes 1572868
  243.0 23.6 %collective-permute-start.13 = (bf16[8,256,128]{2,1,0:T(8,128)(2,1)S(1)}, bf16[8,256,128]{2,1,0:T(8,128)(2,1)S(1)}, u32[]{:S(2)}, u32[]{:S(2)}) collective-permute-start(bf16[8,256,128]{2,1,0:T(8,128)(2,1)S(1)} %all-to-all-done.own), channel_id=1, source_target_pairs={{0,16},{16,0},{1,17},{17,1},{2,18},{18,2},{3,19},{19,3},{4,20},{20... | collective-permute-start | bytes 1572872 | tf_op jit(solution)/shard_map/ppermute | solution.py:90
  245.8 9.7 %copy-start.12 = (f32[2048,256]{1,0:T(8,128)S(1)}, f32[2048,256]{1,0:T(8,128)}, u32[]{:S(2)}) copy-start(f32[2048,256]{1,0:T(8,128)} %param.15) | copy-start | bytes 6291460
  255.5 16.0 %copy-start.1 = (bf16[128,2048]{1,0:T(8,128)(2,1)S(1)}, bf16[128,2048]{1,0:T(8,128)(2,1)}, u32[]{:S(2)}) copy-start(bf16[128,2048]{1,0:T(8,128)(2,1)} %param.10) | copy-start | bytes 1572868
  266.6 0.8 copy-start.18
